TPU v7x, 256 devices: a 4x2x16 block of a 4x16x16 slice. The times are simulated.
256 devices in a mesh: grp: 2 (over y), tp: 16 (over z), dp: 8 (over x, core).
Axes of the slice: x: 4, y: 2, z: 16, core: 2. Of those that a mesh axis runs over, the one named last changes fastest.
The devices are a block of a 4x16x16 slice.
Arguments:
- tokens: bfloat16 [512, 4096], P('grp', 'dp'), parts along dimension 0, may hold values from -40 to 40
- sequence_lengths: int32 [512], P(('grp', 'dp')), parts along dimension 0, may hold values from 1 to 4096, 262144 in all
- recurrent_state: float32 [2, 512, 128, 128], P(None, ('grp', 'dp'), 'tp'), parts along dimension 1, may hold values from -1.8 to 1.8
- norm_weight: float32 [2, 4096], P(None, 'dp'), may hold values from 0.1 to 1.9
- input_weight: bfloat16 [2, 4096, 2048], P(None, 'dp', 'tp'), may hold values from -0.09375 to 0.09375
- gate_weight: bfloat16 [2, 4096, 2048], P(None, 'dp', 'tp'), may hold values from -0.09375 to 0.09375
- output_weight: bfloat16 [2, 2048, 4096], P(None, 'tp', 'dp'), may hold values from -0.125 to 0.125
- negated_real_rate: float32 [2, 8192], P(None, 'tp'), may hold values from 0.005 to 1
- frequency: float32 [2, 8192], P(None, 'tp'), may hold values from -4 to 4
- discrete_step: float32 [2, 128], P(None, 'tp'), may hold values from 0.02 to 0.5
- group_input_matrix: float32 [2, 128, 16, 128], P(None, 'tp'), may hold values from -1.5 to 1.5
- group_output_matrix: float32 [2, 128, 16, 128], P(None, 'tp'), may hold values from -0.5 to 0.5
- feedthrough_weight: float32 [2, 2048], P(None, 'tp'), may hold values from -3 to 3
- extra_log_decay: float32 [2, 128, 4096], P(None, 'tp'), may hold values from -0.7 to 0
Outputs:
- tokens_out: bfloat16 [512, 4096], P('grp', 'dp'), parts along dimension 0
- state_out: float32 [2, 512, 128, 128], P(None, ('grp', 'dp'), 'tp'), parts along dimension 1
There are 2 independent parts, one for each index of `grp`. A program takes and returns all parts, laid end to end along the dimension named above; an argument that names none is the same for every part. Nothing has to cross between parts.
Inputs may be any that keep to these rules, and one draw needn't show every extreme that they name: The newest token of a sequence stands at position sequence_lengths - 1.
All inputs are finite; a program needn't handle non-finite values. No bound on the sum of `sequence_lengths` on one device may be relied on, other than what follows from the above.
Results may differ from a plain program's by a relative error of at most 0.009.
Values may be sent and summed in bfloat16 or wider, within the bound.
A program may use at most 64 MiB of HBM per device.

v0:
```python
import jax
import jax.numpy as jnp
from jax import lax
from jax.sharding import PartitionSpec as P

D = 4096
STACKED_LAYERS = 2


TOP_PRECISION = lax.Precision.HIGHEST
NORM_EPS = 1e-06


def in_blocks(array, dim, peers):
    shape = array.shape
    pieces = array.reshape(*shape[:dim], peers, shape[dim] // peers, *shape[dim + 1 :])
    return jnp.moveaxis(pieces, dim, 0)


def summed_on_arrival(array, axis, dim):
    peers = lax.axis_size(axis)
    pieces = lax.all_to_all(in_blocks(array, dim, peers), axis, 0, 0, tiled=True)
    return jnp.sum(pieces, axis=0)


def in_one_piece(arrays, axis, dim, along):
    columns = [a.reshape(*a.shape[:along], -1) for a in arrays]
    both = jnp.concatenate(columns, axis=along)
    out, at, outs = (summed_on_arrival(both, axis, dim), 0, [])
    for a, column in zip(arrays, columns):
        share = out[..., at : at + column.shape[along]]
        outs.append(share.reshape(*share.shape[:along], *a.shape[along:]))
        at += column.shape[along]
    return tuple(outs)


def laid_out(pieces, dim):
    pieces = jnp.moveaxis(pieces, 0, dim)
    shape = pieces.shape
    return pieces.reshape(*shape[:dim], shape[dim] * shape[dim + 1], *shape[dim + 2 :])


def copy_for_each(array, axis):
    copies = jnp.broadcast_to(array, (lax.axis_size(axis), *array.shape))
    return lax.all_to_all(copies, axis, split_axis=0, concat_axis=0, tiled=True)


def gather_directly(array, axis, dim):
    return laid_out(copy_for_each(array, axis), dim)


def sent_and_summed(array, axis, dim):
    peers = lax.axis_size(axis)
    pieces = lax.all_to_all(in_blocks(array, dim, peers), axis, 0, 0, tiled=True)
    return jnp.sum(pieces.astype(jnp.float32), axis=0)


def transition(decay_factor, angular_frequency, step_width):
    log_mag = -decay_factor * step_width[:, None]
    turn = angular_frequency * step_width[:, None]
    magnitude = jnp.exp(log_mag)
    discrete_real = magnitude * jnp.cos(turn)
    discrete_imaginary = magnitude * jnp.sin(turn)
    half_sine = jnp.sin(0.5 * turn)
    numer_re = jnp.expm1(log_mag) * jnp.cos(turn) - 2.0 * half_sine * half_sine
    denom = decay_factor * decay_factor + angular_frequency * angular_frequency
    drive_re = (-numer_re * decay_factor + discrete_imaginary * angular_frequency) / denom
    drive_im = (-discrete_imaginary * decay_factor - numer_re * angular_frequency) / denom
    return (discrete_real, discrete_imaginary, drive_re, drive_im)


def state_space_update(
    input_groups,
    layer_state,
    extra_decay_factor,
    decay_factor,
    angular_frequency,
    step_width,
    input_matrix,
    readout_matrix,
):
    half_width = input_matrix.shape[-1] // 2
    decay_factor = decay_factor.reshape(-1, half_width)
    angular_frequency = angular_frequency.reshape(-1, half_width)
    discrete_real, discrete_imaginary, drive_re, drive_im = transition(
        decay_factor, angular_frequency, step_width
    )
    input_real = input_matrix[..., :half_width]
    input_imaginary = input_matrix[..., half_width:]
    driven_input_real = jnp.einsum(
        "tkl,klf->tkf", input_groups, input_real, precision=TOP_PRECISION
    )
    driven_input_imaginary = jnp.einsum(
        "tkl,klf->tkf", input_groups, input_imaginary, precision=TOP_PRECISION
    )
    state_re = layer_state[..., :half_width]
    state_im = layer_state[..., half_width:]
    carried_real = extra_decay_factor[..., None] * discrete_real[None]
    carried_imaginary = extra_decay_factor[..., None] * discrete_imaginary[None]
    updated_real = (
        carried_real * state_re
        - carried_imaginary * state_im
        + drive_re[None] * driven_input_real
        - drive_im[None] * driven_input_imaginary
    )
    updated_imaginary = (
        carried_real * state_im
        + carried_imaginary * state_re
        + drive_re[None] * driven_input_imaginary
        + drive_im[None] * driven_input_real
    )
    readout_rows = jnp.einsum(
        "hzk,dhk->dhz", readout_matrix[..., :half_width], updated_real, precision=TOP_PRECISION
    ) - jnp.einsum(
        "hzk,dhk->dhz", readout_matrix[..., half_width:], updated_imaginary, precision=TOP_PRECISION
    )
    return (readout_rows, jnp.concatenate([updated_real, updated_imaginary], axis=-1))


def single_layer(
    hidden_rows,
    sequence_lengths,
    layer_state,
    norm_scale_rows,
    input_matrix_weight,
    gate_matrix,
    output_matrix_weight,
    decay_factor,
    angular_frequency,
    step_width,
    input_matrix,
    readout_matrix,
    feedthrough_rows,
    extra_decay_rows,
):
    x_float = hidden_rows.astype(jnp.float32)
    square_sums = jnp.sum(x_float * x_float, axis=1)
    scaled_in = (x_float * norm_scale_rows[None, :]).astype(jnp.bfloat16)
    input_part = jnp.dot(scaled_in, input_matrix_weight, preferred_element_type=jnp.float32)
    gate_part = jnp.dot(scaled_in, gate_matrix, preferred_element_type=jnp.float32)
    local_rows = sequence_lengths.shape[0]
    input_sum, gate_sum, mine_squares = in_one_piece(
        (input_part, gate_part, square_sums), "dp", 0, 1
    )
    scale = lax.rsqrt(mine_squares / D + NORM_EPS)[:, None]
    u_vals = (input_sum * scale).astype(jnp.bfloat16)
    gate_vals = (gate_sum * scale).astype(jnp.bfloat16)
    group_count = layer_state.shape[1]
    input_float = u_vals.astype(jnp.float32)
    token_positions = sequence_lengths - 1
    extra_decay_factor = jnp.exp(jnp.take(extra_decay_rows, token_positions, axis=1).T)
    readout_rows, updated_state = state_space_update(
        input_float.reshape(local_rows, group_count, -1),
        layer_state,
        extra_decay_factor,
        decay_factor,
        angular_frequency,
        step_width,
        input_matrix,
        readout_matrix,
    )
    y_vals = jax.nn.gelu(
        readout_rows.reshape(local_rows, -1) + feedthrough_rows[None, :] * input_float
    )
    mixed = (y_vals * jax.nn.sigmoid(gate_vals.astype(jnp.float32))).astype(jnp.bfloat16)
    branch_terms = jnp.dot(
        gather_directly(mixed, "dp", 0), output_matrix_weight, preferred_element_type=jnp.float32
    )
    branch_share = sent_and_summed(branch_terms.astype(jnp.bfloat16), "tp", 0).astype(jnp.bfloat16)
    branch = gather_directly(branch_share, "tp", 0)
    x_next = (x_float + branch.astype(jnp.float32)).astype(jnp.bfloat16)
    return (x_next, updated_state)


def on_device(
    tokens,
    sequence_lengths,
    recurrent_state,
    norm_weight,
    input_weight,
    gate_weight,
    output_weight,
    negated_real_rate,
    frequency,
    discrete_step,
    group_input_matrix,
    group_output_matrix,
    feedthrough_weight,
    extra_log_decay,
):
    hidden_rows = tokens
    states = []
    for index_of_layer in range(STACKED_LAYERS):
        hidden_rows, updated_state = single_layer(
            hidden_rows,
            sequence_lengths,
            recurrent_state[index_of_layer],
            norm_weight[index_of_layer],
            input_weight[index_of_layer],
            gate_weight[index_of_layer],
            output_weight[index_of_layer],
            negated_real_rate[index_of_layer],
            frequency[index_of_layer],
            discrete_step[index_of_layer],
            group_input_matrix[index_of_layer],
            group_output_matrix[index_of_layer],
            feedthrough_weight[index_of_layer],
            extra_log_decay[index_of_layer],
        )
        states.append(updated_state)
    return (hidden_rows, jnp.stack(states, axis=0))


def solution(mesh):
    in_specs = (
        P("grp", "dp"),
        P(("grp", "dp")),
        P(None, ("grp", "dp"), "tp", None),
        P(None, "dp"),
        P(None, "dp", "tp"),
        P(None, "dp", "tp"),
        P(None, "tp", "dp"),
        P(None, "tp"),
        P(None, "tp"),
        P(None, "tp"),
        P(None, "tp", None, None),
        P(None, "tp", None, None),
        P(None, "tp"),
        P(None, "tp", None),
    )
    out_specs = (P("grp", "dp"), P(None, ("grp", "dp"), "tp", None))
    return jax.shard_map(
        on_device, mesh=mesh, in_specs=in_specs, out_specs=out_specs, check_vma=False
    )
```

profile of v0, /device:TPU:40, one launch (start us, length us, event | category | flops | bytes accessed | tf_op | source)
XLA Modules:
  0.0 175.1 jit_solution(14124184938763455528)
XLA Ops:
  0.7 1.4 fusion.84
  2.1 1.1 fusion
  3.2 1.1 fusion.24
  4.3 1.1 fusion.26
  5.6 0.8 pad_maximum_fusion
  6.4 4.6 %all-to-all-start = ((f32[8,32,257]{2,1,0:T(8,128)}), f32[8,32,257]{2,1,0:T(8,128)S(1)}, u32[]{:S(2)}, u32[]{:S(2)}) async-start(f32[8,32,257]{2,1,0:T(8,128)} %pad_maximum_fusion), calls=%async_computation | async-start | bytes 786432 | tf_op jit(solution)/shard_map/all_to_all | solution.py:22
  11.0 0.6 slice_reduce_fusion
  11.6 0.7 reshape_squeeze.12
  12.3 0.7 reshape_squeeze.13
  13.0 0.6 slice_bitcast_fusion.5
  13.6 0.5 compare_and_fusion
  14.1 0.6 pad_clamp_fusion
  14.7 0.6 copy.64
  15.3 1.9 %copy.66 = f32[1,8,4096]{1,2,0:T(8,128)} copy(f32[1,8,4096]{2,1,0:T(8,128)S(1)} %get-tuple-element.23) | data formatting | bytes 262144
  17.3 0.8 gather_fusion
  18.1 2.3 %gather_fusion.1 = f32[32,8]{1,0:T(8,128)S(1)} fusion(f32[8,4096]{0,1:T(8,128)} %bitcast.123, s32[1024]{0:T(1024)} %pad_clamp_fusion), kind=kCustom, calls=%fused_computation.1.clone | custom fusion | bytes 2176 | tf_op jit(solution)/shard_map/jit(_take)/gather | solution.py:151
  20.5 0.8 exponential_multiply_fusion.1
  21.3 0.7 fusion.76
  22.0 0.8 slice_bitcast_fusion.4
  24.8 10.2 %all_to_all.40 = bf16[8,32,128]{2,1,0:T(8,128)(2,1)S(1)} all-to-all(bf16[8,32,128]{2,1,0:T(8,128)(2,1)S(1)} %broadcast_in_dim.17), channel_id=1, replica_groups=mesh['grp'=2,'tp'=16,'dp'=8] {'dp'}, dimensions={0} | all-to-all | bytes 131072 | tf_op jit(solution)/shard_map/all_to_all | solution.py:45
  35.2 42.1 %all_to_all.41 = bf16[16,16,512]{2,1,0:T(8,128)(2,1)S(1)} all-to-all(bf16[16,16,512]{2,1,0:T(8,128)(2,1)S(1)} %bitcast.124), channel_id=1, replica_groups=mesh['grp'=2,'tp'=16,'dp'=8] {'tp'}, dimensions={0} | all-to-all | bytes 524288 | tf_op jit(solution)/shard_map/all_to_all | solution.py:54
  77.4 23.9 %all_to_all.42 = bf16[16,16,512]{2,1,0:T(8,128)(2,1)S(1)} all-to-all(bf16[16,16,512]{2,1,0:T(8,128)(2,1)S(1)} %broadcast_in_dim.18), channel_id=1, replica_groups=mesh['grp'=2,'tp'=16,'dp'=8] {'tp'}, dimensions={0} | all-to-all | bytes 524288 | tf_op jit(solution)/shard_map/all_to_all | solution.py:45
  102.2 0.8 pad_maximum_fusion.1
  102.9 3.7 %all-to-all-start.4 = ((f32[8,32,257]{2,1,0:T(8,128)}), f32[8,32,257]{2,1,0:T(8,128)S(1)}, u32[]{:S(2)}, u32[]{:S(2)}) async-start(f32[8,32,257]{2,1,0:T(8,128)} %pad_maximum_fusion.1), calls=%async_computation.4 | async-start | bytes 786432 | tf_op jit(solution)/shard_map/all_to_all | solution.py:22
  107.0 8.3 %all-to-all-done.4 = f32[8,32,257]{2,1,0:T(8,128)S(1)} async-done(((f32[8,32,257]{2,1,0:T(8,128)}), f32[8,32,257]{2,1,0:T(8,128)S(1)}, u32[]{:S(2)}, u32[]{:S(2)}) %all-to-all-start.4) | async-done | bytes 263200 | tf_op jit(solution)/shard_map/all_to_all | solution.py:22
  117.2 8.1 %all_to_all.43 = bf16[8,32,128]{2,1,0:T(8,128)(2,1)S(1)} all-to-all(bf16[8,32,128]{2,1,0:T(8,128)(2,1)S(1)} %broadcast_in_dim.19), channel_id=1, replica_groups=mesh['grp'=2,'tp'=16,'dp'=8] {'dp'}, dimensions={0} | all-to-all | bytes 131072 | tf_op jit(solution)/shard_map/all_to_all | solution.py:45
  125.5 23.9 %all_to_all.44 = bf16[16,16,512]{2,1,0:T(8,128)(2,1)S(1)} all-to-all(bf16[16,16,512]{2,1,0:T(8,128)(2,1)S(1)} %bitcast.125), channel_id=1, replica_groups=mesh['grp'=2,'tp'=16,'dp'=8] {'tp'}, dimensions={0} | all-to-all | bytes 524288 | tf_op jit(solution)/shard_map/all_to_all | solution.py:54
  149.4 0.7 broadcast_in_dim.20
  150.1 5.8 %all-to-all-start.7 = ((bf16[16,16,512]{2,1,0:T(8,128)(2,1)}), bf16[16,16,512]{2,1,0:T(8,128)(2,1)S(1)}, u32[]{:S(2)}, u32[]{:S(2)}) async-start(bf16[16,16,512]{2,1,0:T(8,128)(2,1)} %broadcast_in_dim.20), calls=%async_computation.7 | async-start | bytes 524288 | tf_op jit(solution)/shard_map/all_to_all | solution.py:45
  156.2 0.9 copy.63
  157.0 17.2 %all-to-all-done.7 = bf16[16,16,512]{2,1,0:T(8,128)(2,1)S(1)} async-done(((bf16[16,16,512]{2,1,0:T(8,128)(2,1)}), bf16[16,16,512]{2,1,0:T(8,128)(2,1)S(1)}, u32[]{:S(2)}, u32[]{:S(2)}) %all-to-all-start.7) | async-done | bytes 262176 | tf_op jit(solution)/shard_map/all_to_all | solution.py:45
  174.2 0.8 fusion.5
  (78 shorter events, 6.1 us)
Async XLA Ops:
  0.6 10.3 %copy-start.6 = (f32[2,8,16,128]{3,2,1,0:T(8,128)S(1)}, f32[2,8,16,128]{3,2,1,0:T(8,128)}, u32[]{:S(2)}) copy-start(f32[2,8,16,128]{3,2,1,0:T(8,128)} %param.26) | copy-start | bytes 393220
  0.6 10.4 %copy-start.12 = (f32[2,512]{1,0:T(2,128)S(1)}, f32[2,512]{1,0:T(2,128)}, u32[]{:S(2)}) copy-start(f32[2,512]{1,0:T(2,128)} %param.23) | copy-start | bytes 12292
  0.7 10.4 %copy-start.11 = (f32[2,512]{1,0:T(2,128)S(1)}, f32[2,512]{1,0:T(2,128)}, u32[]{:S(2)}) copy-start(f32[2,512]{1,0:T(2,128)} %param.24) | copy-start | bytes 12292
  0.7 12.3 %copy-start.14 = (f32[2,8]{1,0:T(2,128)S(1)}, f32[2,8]{1,0:T(2,128)}, u32[]{:S(2)}) copy-start(f32[2,8]{1,0:T(2,128)} %param.25) | copy-start | bytes 196
  0.7 12.9 %copy-start.15 = (s32[32]{0:T(128)S(1)}, s32[32]{0:T(128)}, u32[]{:S(2)}) copy-start(s32[32]{0:T(128)} %param.17) | copy-start | bytes 388
  0.7 14.0 %copy-start.2 = (f32[2,8,4096]{2,1,0:T(8,128)S(1)}, f32[2,8,4096]{2,1,0:T(8,128)}, u32[]{:S(2)}) copy-start(f32[2,8,4096]{2,1,0:T(8,128)} %param.29) | copy-start | bytes 786436
  6.4 16.4 %all-to-all-start = ((f32[8,32,257]{2,1,0:T(8,128)}), f32[8,32,257]{2,1,0:T(8,128)S(1)}, u32[]{:S(2)}, u32[]{:S(2)}) async-start(f32[8,32,257]{2,1,0:T(8,128)} %pad_maximum_fusion), calls=%async_computation | async-start | bytes 786432 | tf_op jit(solution)/shard_map/all_to_all | solution.py:22
  14.7 5.7 %copy-start.3 = (f32[2,32,8,128]{3,2,1,0:T(8,128)S(1)}, f32[2,32,8,128]{3,2,1,0:T(8,128)}, u32[]{:S(2)}) copy-start(f32[2,32,8,128]{3,2,1,0:T(8,128)} %param.18) | copy-start | bytes 786436
  15.3 7.5 %copy-start.7 = (f32[2,8,16,128]{3,2,1,0:T(8,128)S(1)}, f32[2,8,16,128]{3,2,1,0:T(8,128)}, u32[]{:S(2)}) copy-start(f32[2,8,16,128]{3,2,1,0:T(8,128)} %param.27) | copy-start | bytes 393220
  17.3 17.8 %copy-start.1 = (bf16[2,128,512]{2,1,0:T(8,128)(2,1)S(1)}, bf16[2,128,512]{2,1,0:T(8,128)(2,1)}, u32[]{:S(2)}) copy-start(bf16[2,128,512]{2,1,0:T(8,128)(2,1)} %param.22) | copy-start | bytes 786436
  22.9 78.4 %copy-start = (bf16[256,512]{1,0:T(8,128)(2,1)S(1)}, bf16[256,512]{1,0:T(8,128)(2,1)}, u32[]{:S(2)}) copy-start(bf16[256,512]{1,0:T(8,128)(2,1)} %param.16) | copy-start | bytes 786436
  22.9 78.4 %copy-start.8 = (f32[1,512]{1,0:T(1,128)S(1)}, f32[1,512]{1,0:T(1,128)}, u32[]{:S(2)}) copy-start(f32[1,512]{1,0:T(1,128)} %get-tuple-element.41) | copy-start | bytes 6148
  23.6 77.9 %copy-start.4 = (bf16[2,512,128]{2,1,0:T(8,128)(2,1)S(1)}, bf16[2,512,128]{2,1,0:T(8,128)(2,1)}, u32[]{:S(2)}) copy-start(bf16[2,512,128]{2,1,0:T(8,128)(2,1)} %param.21) | copy-start | bytes 786436
  24.2 77.5 %copy-start.5 = (bf16[2,512,128]{2,1,0:T(8,128)(2,1)S(1)}, bf16[2,512,128]{2,1,0:T(8,128)(2,1)}, u32[]{:S(2)}) copy-start(bf16[2,512,128]{2,1,0:T(8,128)(2,1)} %param.20) | copy-start | bytes 786436
  77.4 29.2 %copy-start.10 = (f32[512]{0:T(512)S(1)}, f32[512]{0:T(512)}, u32[]{:S(2)}) copy-start(f32[512]{0:T(512)} %get-tuple-element.52) | copy-start | bytes 6148
  77.4 29.3 %copy-start.9 = (f32[512]{0:T(512)S(1)}, f32[512]{0:T(512)}, u32[]{:S(2)}) copy-start(f32[512]{0:T(512)} %get-tuple-element.13) | copy-start | bytes 6148
  77.4 29.5 %copy-start.13 = (f32[8]{0:T(128)S(1)}, f32[8]{0:T(128)}, u32[]{:S(2)}) copy-start(f32[8]{0:T(128)} %get-tuple-element.45) | copy-start | bytes 100
  102.9 12.4 %all-to-all-start.4 = ((f32[8,32,257]{2,1,0:T(8,128)}), f32[8,32,257]{2,1,0:T(8,128)S(1)}, u32[]{:S(2)}, u32[]{:S(2)}) async-start(f32[8,32,257]{2,1,0:T(8,128)} %pad_maximum_fusion.1), calls=%async_computation.4 | async-start | bytes 786432 | tf_op jit(solution)/shard_map/all_to_all | solution.py:22
  150.1 24.1 %all-to-all-start.7 = ((bf16[16,16,512]{2,1,0:T(8,128)(2,1)}), bf16[16,16,512]{2,1,0:T(8,128)(2,1)S(1)}, u32[]{:S(2)}, u32[]{:S(2)}) async-start(bf16[16,16,512]{2,1,0:T(8,128)(2,1)} %broadcast_in_dim.20), calls=%async_computation.7 | async-start | bytes 524288 | tf_op jit(solution)/shard_map/all_to_all | solution.py:45
where the time goes:
time: 176 us; the launch traced here: 175 us
  blocking collectives  108 us (61%)
  waiting for transfers between devices  25.6 us (15%)
  starting transfers between devices  14 us (8%)
  local copies, waits for them, and re-layouts  13.2 us (8%)
  other arithmetic  7.39 us (4%)
  matrix products  5.73 us (3%)
    all_to_all x2, blocking collectives, sent_and_summed(): lax.all_to_all(in_blocks(array, dim, peers), axis, 0, 0, tiled=True)  65.9 us
    all_to_all x3, blocking collectives, copy_for_each(): return lax.all_to_all(copies, axis, split_axis=0, concat_axis=0, tiled=True)  42.2 us
    all_to_all x1, waiting for transfers between devices, copy_for_each(): return lax.all_to_all(copies, axis, split_axis=0, concat_axis=0, tiled=True)  17.2 us
    all_to_all x2, waiting for transfers between devices, summed_on_arrival(): lax.all_to_all(in_blocks(array, dim, peers), axis, 0, 0, tiled=True)  8.33 us
    all_to_all x2, starting transfers between devices, summed_on_arrival(): lax.all_to_all(in_blocks(array, dim, peers), axis, 0, 0, tiled=True)  8.24 us
    all_to_all x1, starting transfers between devices, copy_for_each(): return lax.all_to_all(copies, axis, split_axis=0, concat_axis=0, tiled=True)  5.77 us
  transfers between devices with their start and end apart: 3, of which 2 were waited for; matrix products, arithmetic and copies ran while one was open for 8% of the time, Pallas kernels for 0%

commit v1 on v0

v1 whole, which is shorter than its diff:
```python
import functools

import jax
import jax.numpy as jnp
from jax import lax
from jax.experimental import pallas as pl
from jax.experimental.pallas import tpu as pltpu
from jax.sharding import PartitionSpec as P

NORM_EPS = 1e-06
HIGHEST = lax.Precision.HIGHEST
F32 = jnp.float32
BF16 = jnp.bfloat16
MESH = pl.DeviceIdType.MESH


def contract_last(a, b, precision=None):
    return lax.dot_general(
        a, b, (((1,), (1,)), ((), ())), precision=precision, preferred_element_type=F32
    )


def split_two(a):
    high = a.astype(BF16)
    return high, (a - high.astype(F32)).astype(BF16)


def exp_less_one(x, exp_x):
    series = jnp.full_like(x, 1.0 / 3628800.0)
    for factor in (362880.0, 40320.0, 5040.0, 720.0, 120.0, 24.0, 6.0, 2.0, 1.0):
        series = series * x + 1.0 / factor
    return jnp.where(jnp.abs(x) < 0.6, series * x, exp_x - 1.0)


def kernel(
    n_dp,
    n_tp,
    features,
    lengths,
    step_width,
    tokens_hbm,
    norm_hbm,
    w_in_hbm,
    w_gate_hbm,
    decay_hbm,
    state_hbm,
    rate_hbm,
    freq_hbm,
    b_hbm,
    c_hbm,
    feed_hbm,
    w_out_hbm,
    tokens_out,
    state_out,
    x_buf,
    norm,
    w_cat,
    w_out,
    decay,
    state,
    rate,
    freq,
    b_mat,
    c_mat,
    feed,
    local_sem,
    out_sem,
    part_buf,
    part_recv,
    part_send_sem,
    part_recv_sem,
    sq_buf,
    sq_recv,
    sq_send_sem,
    sq_recv_sem,
    z_buf,
    z_send_sem,
    z_recv_sem,
    term_buf,
    term_recv,
    term_send_sem,
    term_recv_sem,
    x_send_sem,
    x_recv_sem,
    pick,
    carried,
    drive_high,
    drive_low,
    mix_cat,
    base,
):
    i = lax.axis_index("dp")
    j = lax.axis_index("tp")
    layers, mine, groups, width = state.shape
    half = width // 2
    rows, local_d = x_buf.shape[1:]
    chans = w_out.shape[1]
    chunk = rows // n_tp
    per_block = mine // chunk
    channel_group = chans // groups

    dp_steps = [(0, 1)] + [
        (d, e) for d in (1, n_dp // 2 - 1, 2) for e in (0, 1)
    ]

    def dp_peer(step):
        d, e = step
        return lax.rem(lax.div(i, 2) + d, n_dp // 2) * 2 + lax.rem(lax.rem(i, 2) + e, 2)

    tp_steps = []
    for d in range(1, n_tp // 2 + 1):
        tp_steps.append(d)
        if n_tp - d != d:
            tp_steps.append(n_tp - d)

    def tp_peer(step):
        return lax.rem(j + step, n_tp)

    barrier = pltpu.get_barrier_semaphore()
    for step in dp_steps:
        pl.semaphore_signal(barrier, inc=1, device_id={"dp": dp_peer(step)}, device_id_type=MESH)
    for step in tp_steps:
        pl.semaphore_signal(barrier, inc=1, device_id={"tp": tp_peer(step)}, device_id_type=MESH)

    loads = {}
    for n, (name, src, dst) in enumerate(
        [
            ("x", tokens_hbm, x_buf.at[0]),
            ("norm", norm_hbm, norm),
            ("w_in", w_in_hbm, w_cat.at[:, :, pl.ds(0, chans)]),
            ("w_gate", w_gate_hbm, w_cat.at[:, :, pl.ds(chans, chans)]),
            ("decay", decay_hbm, decay),
            ("state", state_hbm, state),
            ("rate", rate_hbm, rate),
            ("freq", freq_hbm, freq),
            ("b", b_hbm, b_mat),
            ("c", c_hbm, c_mat),
            ("feed", feed_hbm, feed),
            ("w_out", w_out_hbm, w_out),
        ]
    ):
        loads[name] = pltpu.make_async_copy(src, dst, local_sem.at[n])
        loads[name].start()

    lane = lax.broadcasted_iota(jnp.int32, (groups, width), 1)
    sub = lax.broadcasted_iota(jnp.int32, (groups, width), 0)
    low = lane < half
    col_group = lax.broadcasted_iota(jnp.int32, (groups, chans), 1) // channel_group
    own_group = col_group == lax.broadcasted_iota(jnp.int32, (groups, chans), 0)
    block_row = lax.broadcasted_iota(jnp.int32, (chans, chans), 0) // channel_group
    block_col = lax.broadcasted_iota(jnp.int32, (chans, chans), 1) // channel_group

    def by_group(ref, layer):
        out = jnp.zeros((groups, width), F32)
        for g in range(groups):
            pair = ref[layer : layer + 1, (g // 2) * width : (g // 2 + 1) * width]
            other = pltpu.roll(pair, half, 1)
            row = jnp.where(low[:1] if g % 2 == 0 else ~low[:1], pair, other)
            out = jnp.where(sub == g, row, out)
        return out

    def prepare(layer):
        dt = jnp.zeros((groups, width), F32)
        for g in range(groups):
            dt = jnp.where(sub == g, step_width[layer, g], dt)
        a_re = by_group(rate, layer)
        a_im = by_group(freq, layer)
        log_mag = -a_re * dt
        turn = a_im * dt
        magnitude = jnp.exp(log_mag)
        cosine = jnp.cos(turn)
        disc_re = magnitude * cosine
        disc_im = magnitude * jnp.sin(turn)
        half_sine = jnp.sin(0.5 * turn)
        numer_re = exp_less_one(log_mag, magnitude) * cosine - 2.0 * half_sine * half_sine
        denom = a_re * a_re + a_im * a_im
        drive_re = (-numer_re * a_re + disc_im * a_im) / denom
        drive_im = (-disc_im * a_re - numer_re * a_im) / denom
        disc_cross = jnp.where(low, -disc_im, disc_im)
        drive_cross = jnp.where(low, -drive_im, drive_im)

        b_l = b_mat[layer]
        drive = drive_re[:, None, :] * b_l + drive_cross[:, None, :] * pltpu.roll(b_l, half, 2)
        drive = drive.reshape(chans, width)
        high, rest = split_two(drive)
        drive_high[layer] = high
        drive_low[layer] = rest
        c_l = jnp.where(low[:1][None], c_mat[layer], -c_mat[layer]).reshape(chans, width)
        mix = jnp.where(block_row == block_col, contract_last(drive, c_l, HIGHEST), 0.0)
        high, rest = split_two(mix)
        mix_cat[layer, :chans] = high
        mix_cat[layer, chans:] = rest

        for r in range(mine):
            offset = lane - (lengths[r] - 1)
            found = jnp.zeros((groups, width), F32)
            for at in range(0, decay.shape[2], width):
                found = jnp.where(offset == -at, decay[layer, :, at : at + width], found)
            pick[r] = found
        extra = jnp.exp(jnp.sum(pick[...], axis=-1, keepdims=True))
        s = state[layer]
        kept = extra * (disc_re[None] * s + disc_cross[None] * pltpu.roll(s, half, 2))
        carried[layer] = kept
        read = contract_last(kept.reshape(mine * groups, width), c_l, HIGHEST)
        read = jnp.where(own_group[None], read.reshape(mine, groups, chans), 0.0)
        base[layer] = jnp.sum(read, axis=1)

    def send_part(layer, s):
        for src, dst, ssem, rsem in (
            (part_buf, part_recv, part_send_sem, part_recv_sem),
            (sq_buf, sq_recv, sq_send_sem, sq_recv_sem),
        ):
            pltpu.make_async_remote_copy(
                src_ref=src.at[layer, s],
                dst_ref=dst.at[layer, i],
                send_sem=ssem.at[layer, s],
                recv_sem=rsem.at[layer, i],
                device_id={"dp": s},
                device_id_type=MESH,
            ).start()

    ones = jnp.ones((8, 128), F32)

    def square_rows(x):
        x2 = x * x
        total = x2[:, 0:128]
        for k in range(1, local_d // 128):
            total = total + x2[:, k * 128 : (k + 1) * 128]
        return contract_last(ones, total, HIGHEST)

    sends = []

    loads["x"].wait()
    loads["norm"].wait()
    x = x_buf[0].astype(F32)
    scaled = (x * norm[0:1, :]).astype(BF16)
    squares = square_rows(x)
    for s in range(n_dp):
        sq_buf[0, s, :, pl.ds(0, mine)] = squares[:, s * mine : (s + 1) * mine]
    loads["w_in"].wait()
    loads["w_gate"].wait()
    part_buf[0] = (
        jnp.dot(scaled, w_cat[0], preferred_element_type=F32)
        .astype(BF16)
        .reshape(n_dp, mine, 2 * chans)
    )
    for name in ("decay", "state", "rate", "freq", "b", "c", "feed", "w_out"):
        loads[name].wait()
    pl.semaphore_wait(barrier, len(dp_steps) + len(tp_steps))
    for step in dp_steps:
        send_part(0, dp_peer(step))
    for layer in range(layers):
        prepare(layer)

    row_lane = lax.broadcasted_iota(jnp.int32, (mine, 128), 1)
    row_sub = lax.broadcasted_iota(jnp.int32, (mine, 128), 0)

    for layer in range(layers):
        total = part_buf[layer, i].astype(F32)
        sq = sq_buf[layer, i]
        for step in dp_steps:
            s = dp_peer(step)
            for src, dst, ssem, rsem in (
                (part_buf, part_recv, part_send_sem, part_recv_sem),
                (sq_buf, sq_recv, sq_send_sem, sq_recv_sem),
            ):
                pltpu.make_async_remote_copy(
                    src_ref=src.at[layer, s],
                    dst_ref=dst.at[layer, s],
                    send_sem=ssem.at[layer, s],
                    recv_sem=rsem.at[layer, s],
                    device_id={"dp": s},
                    device_id_type=MESH,
                ).wait_recv()
            total = total + part_recv[layer, s].astype(F32)
            sq = sq + sq_recv[layer, s]
        mean = jnp.sum(
            jnp.where(row_lane == row_sub, sq[0:1, :], 0.0), axis=1, keepdims=True
        ) / features
        scale = lax.rsqrt(mean + NORM_EPS)
        total = total * scale
        u = total[:, :chans].astype(BF16)
        gate = total[:, chans:].astype(BF16).astype(F32)
        u_f = u.astype(F32)
        read = base[layer] + jnp.dot(
            jnp.concatenate([u, u], axis=1), mix_cat[layer], preferred_element_type=F32
        )
        y = jax.nn.gelu(read + feed[layer : layer + 1, :] * u_f)
        z_buf[layer, i] = (y * jax.nn.sigmoid(gate)).astype(BF16)
        for step in dp_steps:
            s = dp_peer(step)
            pltpu.make_async_remote_copy(
                src_ref=z_buf.at[layer, i],
                dst_ref=z_buf.at[layer, i],
                send_sem=z_send_sem.at[layer, s],
                recv_sem=z_recv_sem.at[layer, i],
                device_id={"dp": s},
                device_id_type=MESH,
            ).start()

        for step in [(0, 0)] + dp_steps:
            s = dp_peer(step)
            if step != (0, 0):
                pltpu.make_async_remote_copy(
                    src_ref=z_buf.at[layer, s],
                    dst_ref=z_buf.at[layer, s],
                    send_sem=z_send_sem.at[layer, s],
                    recv_sem=z_recv_sem.at[layer, s],
                    device_id={"dp": s},
                    device_id_type=MESH,
                ).wait_recv()
            terms = jnp.dot(z_buf[layer, s], w_out[layer], preferred_element_type=F32)
            for k in range(per_block):
                t = s * per_block + k
                term_buf[layer, t] = terms[k * chunk : (k + 1) * chunk].astype(BF16)

                @pl.when(t != j)
                def _():
                    pltpu.make_async_remote_copy(
                        src_ref=term_buf.at[layer, t],
                        dst_ref=term_recv.at[layer, j],
                        send_sem=term_send_sem.at[layer, t],
                        recv_sem=term_recv_sem.at[layer, j],
                        device_id={"tp": t},
                        device_id_type=MESH,
                    ).start()

        spread = jnp.where(own_group[None], u_f[:, None, :], 0.0).astype(BF16)
        spread = spread.reshape(mine * groups, chans)
        driven = jnp.dot(spread, drive_high[layer], preferred_element_type=F32) + jnp.dot(
            spread, drive_low[layer], preferred_element_type=F32
        )
        carried[layer] = carried[layer] + driven.reshape(mine, groups, width)
        pltpu.make_async_copy(carried.at[layer], state_out.at[layer], out_sem.at[layer]).start()

        total = term_buf[layer, j].astype(F32)
        for step in tp_steps:
            t = tp_peer(step)
            pltpu.make_async_remote_copy(
                src_ref=term_buf.at[layer, t],
                dst_ref=term_recv.at[layer, t],
                send_sem=term_send_sem.at[layer, t],
                recv_sem=term_recv_sem.at[layer, t],
                device_id={"tp": t},
                device_id_type=MESH,
            ).wait_recv()
            total = total + term_recv[layer, t].astype(F32)
        at = pl.ds(pl.multiple_of(j * chunk, chunk), chunk)
        branch = total.astype(BF16).astype(F32)
        x_buf[layer + 1, at, :] = (x_buf[layer, at, :].astype(F32) + branch).astype(BF16)
        for step in tp_steps:
            t = tp_peer(step)
            pltpu.make_async_remote_copy(
                src_ref=x_buf.at[layer + 1, at],
                dst_ref=x_buf.at[layer + 1, at],
                send_sem=x_send_sem.at[layer, t],
                recv_sem=x_recv_sem.at[layer, j],
                device_id={"tp": t},
                device_id_type=MESH,
            ).start()

        def await_chunk(t):
            piece = pl.ds(pl.multiple_of(t * chunk, chunk), chunk)
            pltpu.make_async_remote_copy(
                src_ref=x_buf.at[layer + 1, piece],
                dst_ref=x_buf.at[layer + 1, piece],
                send_sem=x_send_sem.at[layer, t],
                recv_sem=x_recv_sem.at[layer, t],
                device_id={"tp": t},
                device_id_type=MESH,
            ).wait_recv()

        if layer + 1 < layers:
            order = [0]
            for d in range(1, n_dp // 2 + 1):
                order.append(d)
                if n_dp - d != d:
                    order.append(n_dp - d)
            for d in order:
                s = lax.rem(lax.div(j, per_block) + d, n_dp)
                for k in range(per_block):
                    t = s * per_block + k
                    if d == 0:
                        pl.when(t != j)(functools.partial(await_chunk, t))
                    else:
                        await_chunk(t)
                piece = pl.ds(pl.multiple_of(s * mine, mine), mine)
                x = x_buf[layer + 1, piece, :].astype(F32)
                scaled = (x * norm[layer + 1 : layer + 2, :]).astype(BF16)
                sq_buf[layer + 1, s, :, pl.ds(0, mine)] = square_rows(x)
                part_buf[layer + 1, s] = jnp.dot(
                    scaled, w_cat[layer + 1], preferred_element_type=F32
                ).astype(BF16)
                pl.when(s != i)(functools.partial(send_part, layer + 1, s))
        else:
            for step in tp_steps:
                await_chunk(tp_peer(step))
            pltpu.make_async_copy(x_buf.at[layers], tokens_out, out_sem.at[layers]).start()

    for layer in range(layers):
        for step in dp_steps:
            s = dp_peer(step)
            for src, dst, ssem, rsem in (
                (part_buf, part_recv, part_send_sem, part_recv_sem),
                (sq_buf, sq_recv, sq_send_sem, sq_recv_sem),
            ):
                pltpu.make_async_remote_copy(
                    src_ref=src.at[layer, s],
                    dst_ref=dst.at[layer, i],
                    send_sem=ssem.at[layer, s],
                    recv_sem=rsem.at[layer, i],
                    device_id={"dp": s},
                    device_id_type=MESH,
                ).wait_send()
            pltpu.make_async_remote_copy(
                src_ref=z_buf.at[layer, i],
                dst_ref=z_buf.at[layer, i],
                send_sem=z_send_sem.at[layer, s],
                recv_sem=z_recv_sem.at[layer, i],
                device_id={"dp": s},
                device_id_type=MESH,
            ).wait_send()
        for step in tp_steps:
            t = tp_peer(step)
            pltpu.make_async_remote_copy(
                src_ref=term_buf.at[layer, t],
                dst_ref=term_recv.at[layer, j],
                send_sem=term_send_sem.at[layer, t],
                recv_sem=term_recv_sem.at[layer, j],
                device_id={"tp": t},
                device_id_type=MESH,
            ).wait_send()
            at = pl.ds(pl.multiple_of(j * chunk, chunk), chunk)
            pltpu.make_async_remote_copy(
                src_ref=x_buf.at[layer + 1, at],
                dst_ref=x_buf.at[layer + 1, at],
                send_sem=x_send_sem.at[layer, t],
                recv_sem=x_recv_sem.at[layer, j],
                device_id={"tp": t},
                device_id_type=MESH,
            ).wait_send()
        pltpu.make_async_copy(carried.at[layer], state_out.at[layer], out_sem.at[layer]).wait()
    pltpu.make_async_copy(x_buf.at[layers], tokens_out, out_sem.at[layers]).wait()


def on_device(
    n_dp,
    n_tp,
    tokens,
    sequence_lengths,
    recurrent_state,
    norm_weight,
    input_weight,
    gate_weight,
    output_weight,
    negated_real_rate,
    frequency,
    discrete_step,
    group_input_matrix,
    group_output_matrix,
    feedthrough_weight,
    extra_log_decay,
):
    layers, mine, groups, width = recurrent_state.shape
    rows, local_d = tokens.shape
    chans = output_weight.shape[1]
    chunk = rows // n_tp
    smem = pl.BlockSpec(memory_space=pltpu.SMEM)
    hbm = pl.BlockSpec(memory_space=pl.ANY)
    dma = pltpu.SemaphoreType.DMA
    like = lambda a: pltpu.VMEM(a.shape, a.dtype)
    scratch = [
        pltpu.VMEM((layers + 1, rows, local_d), BF16),
        like(norm_weight),
        pltpu.VMEM((layers, local_d, 2 * chans), BF16),
        like(output_weight),
        like(extra_log_decay),
        like(recurrent_state),
        like(negated_real_rate),
        like(frequency),
        like(group_input_matrix),
        like(group_output_matrix),
        like(feedthrough_weight),
        dma((12,)),
        dma((layers + 1,)),
        pltpu.VMEM((layers, n_dp, mine, 2 * chans), BF16),
        pltpu.VMEM((layers, n_dp, mine, 2 * chans), BF16),
        dma((layers, n_dp)),
        dma((layers, n_dp)),
        pltpu.VMEM((layers, n_dp, 8, 128), F32),
        pltpu.VMEM((layers, n_dp, 8, 128), F32),
        dma((layers, n_dp)),
        dma((layers, n_dp)),
        pltpu.VMEM((layers, n_dp, mine, chans), BF16),
        dma((layers, n_dp)),
        dma((layers, n_dp)),
        pltpu.VMEM((layers, n_tp, chunk, local_d), BF16),
        pltpu.VMEM((layers, n_tp, chunk, local_d), BF16),
        dma((layers, n_tp)),
        dma((layers, n_tp)),
        dma((layers, n_tp)),
        dma((layers, n_tp)),
        pltpu.VMEM((mine, groups, width), F32),
        pltpu.VMEM((layers, mine, groups, width), F32),
        pltpu.VMEM((layers, chans, width), BF16),
        pltpu.VMEM((layers, chans, width), BF16),
        pltpu.VMEM((layers, 2 * chans, chans), BF16),
        pltpu.VMEM((layers, mine, chans), F32),
    ]
    return pl.pallas_call(
        functools.partial(kernel, n_dp, n_tp, n_dp * local_d),
        out_shape=(
            jax.ShapeDtypeStruct(tokens.shape, tokens.dtype),
            jax.ShapeDtypeStruct(recurrent_state.shape, recurrent_state.dtype),
        ),
        in_specs=[smem, smem] + [hbm] * 12,
        out_specs=(hbm, hbm),
        scratch_shapes=scratch,
        compiler_params=pltpu.CompilerParams(collective_id=0, has_side_effects=True),
    )(
        sequence_lengths,
        discrete_step,
        tokens,
        norm_weight,
        input_weight,
        gate_weight,
        extra_log_decay,
        recurrent_state,
        negated_real_rate,
        frequency,
        group_input_matrix,
        group_output_matrix,
        feedthrough_weight,
        output_weight,
    )


def solution(mesh):
    in_specs = (
        P("grp", "dp"),
        P(("grp", "dp")),
        P(None, ("grp", "dp"), "tp", None),
        P(None, "dp"),
        P(None, "dp", "tp"),
        P(None, "dp", "tp"),
        P(None, "tp", "dp"),
        P(None, "tp"),
        P(None, "tp"),
        P(None, "tp"),
        P(None, "tp", None, None),
        P(None, "tp", None, None),
        P(None, "tp"),
        P(None, "tp", None),
    )
    out_specs = (P("grp", "dp"), P(None, ("grp", "dp"), "tp", None))
    return jax.shard_map(
        functools.partial(on_device, mesh.shape["dp"], mesh.shape["tp"]),
        mesh=mesh,
        in_specs=in_specs,
        out_specs=out_specs,
        check_vma=False,
    )
```

time: 176 us -> 114 us (0.65)
  the two profiles are of different devices: /device:TPU:40 before, /device:TPU:39 now
where the time goes in v1:
time: 114 us
  Pallas kernels  111 us (97%)
  local copies, waits for them, and re-layouts  2.42 us (2%)
    pallas_call x1, Pallas kernels, on_device(): pl.pallas_call(functools.partial(kernel, n_dp, n_tp, n_dp * local_d), out...  111 us
    unnamed x4, local copies, waits for them, and re-layouts  2.42 us

profile of v1, /device:TPU:39, one launch (start us, length us, event | category | flops | bytes accessed | tf_op | source)
XLA Modules:
  0.0 113.7 jit_solution(542255550542709779)
XLA Ops:
  0.6 110.7 %shard_map.149 = (bf16[256,512]{1,0:T(8,128)(2,1)}, f32[2,32,8,128]{3,2,1,0:T(8,128)}) custom-call(s32[32]{0:T(128)} %lengths.1, f32[2,8]{1,0:T(2,128)} %step_width.1, bf16[256,512]{1,0:T(8,128)(2,1)} %tokens_hbm.1, f32[2,512]{1,0:T(2,128)} %norm_hbm.1, bf16[2,512,128]{2,1,0:T(8,128)(2,1)} %w_in_hbm.1, bf16[2,512,128]{2,1,0:T(8,128)(2,1)} %w_gate_hbm.1, ...), custom_call_target="tpu_custom_call" | custom-call | tf_op jit(solution)/shard_map/pallas_call | solution.py:510
  111.3 0.0 copy-start
  111.3 1.7 %copy.18 = bf16[256,512]{1,0:T(8,128)(2,1)} copy(bf16[256,512]{1,0:T(8,128)(2,1)} %get-tuple-element.4) | data formatting | bytes 524288
  113.0 0.0 copy-done
  113.0 0.7 copy.19
Async XLA Ops:
  111.3 1.7 %copy-start = (f32[2,32,8,128]{3,2,1,0:T(8,128)S(1)}, f32[2,32,8,128]{3,2,1,0:T(8,128)}, u32[]{:S(2)}) copy-start(f32[2,32,8,128]{3,2,1,0:T(8,128)} %get-tuple-element.5) | copy-start | bytes 786436

commit v2 on v1

--- a/solution.py
+++ b/solution.py
@@ -30,6 +30,15 @@
     for factor in (362880.0, 40320.0, 5040.0, 720.0, 120.0, 24.0, 6.0, 2.0, 1.0):
         series = series * x + 1.0 / factor
     return jnp.where(jnp.abs(x) < 0.6, series * x, exp_x - 1.0)
+
+
+def sign(o):
+    return 1 if o > 0 else -1
+
+
+def step_to_hub(o):
+    near = (abs(o) + 1) // 3 * 3
+    return abs(o) if near in (0, abs(o)) else abs(o) - near
 
 
 def kernel(
@@ -107,20 +116,24 @@
         d, e = step
         return lax.rem(lax.div(i, 2) + d, n_dp // 2) * 2 + lax.rem(lax.rem(i, 2) + e, 2)
 
-    tp_steps = []
-    for d in range(1, n_tp // 2 + 1):
-        tp_steps.append(d)
-        if n_tp - d != d:
-            tp_steps.append(n_tp - d)
-
-    def tp_peer(step):
-        return lax.rem(j + step, n_tp)
+    side = 1 - 2 * lax.rem(j, 2)
+    far = n_tp // 2
+    hub = far - 2
+    tree = {o: o - sign(o) * step_to_hub(o) for o in range(1 - far, far) if o}
+    children = {p: [o for o in tree if tree[o] == p] for p in [0, *tree]}
+    by_reach = sorted(tree, key=lambda o: (-abs(o), o))
+    leaves = [o for o in by_reach if not children[o]]
+    hubs = [o for o in by_reach if children[o]]
+
+    def at_offset(o):
+        return lax.rem(j + o + n_tp, n_tp)
 
     barrier = pltpu.get_barrier_semaphore()
     for step in dp_steps:
         pl.semaphore_signal(barrier, inc=1, device_id={"dp": dp_peer(step)}, device_id_type=MESH)
-    for step in tp_steps:
-        pl.semaphore_signal(barrier, inc=1, device_id={"tp": tp_peer(step)}, device_id_type=MESH)
+    tp_greeted = sorted({(o - tree[o]) % n_tp for o in tree} | {2, n_tp - 2})
+    for step in tp_greeted:
+        pl.semaphore_signal(barrier, inc=1, device_id={"tp": at_offset(step)}, device_id_type=MESH)
 
     loads = {}
     for n, (name, src, dst) in enumerate(
@@ -228,7 +241,47 @@
             total = total + x2[:, k * 128 : (k + 1) * 128]
         return contract_last(ones, total, HIGHEST)
 
-    sends = []
+    def chunk_rows(t):
+        return pl.ds(pl.multiple_of(t * chunk, chunk), chunk)
+
+    def up(layer, o):
+        hop = 2 * side if o == far else o - tree[o]
+        owner = at_offset(-o)
+        return pltpu.make_async_remote_copy(
+            src_ref=term_buf.at[layer, owner],
+            dst_ref=term_recv.at[layer, o % n_tp],
+            send_sem=term_send_sem.at[layer, o % n_tp],
+            recv_sem=term_recv_sem.at[layer, o % n_tp],
+            device_id={"tp": at_offset(-hop)},
+            device_id_type=MESH,
+        )
+
+    arrived = up
+
+    def down(layer, o, c):
+        owner = chunk_rows(at_offset(-o))
+        slot = lax.rem(c + n_tp, n_tp)
+        return pltpu.make_async_remote_copy(
+            src_ref=x_buf.at[layer + 1, owner],
+            dst_ref=x_buf.at[layer + 1, owner],
+            send_sem=x_send_sem.at[layer, slot],
+            recv_sem=x_recv_sem.at[layer, slot],
+            device_id={"tp": at_offset(c - o)},
+            device_id_type=MESH,
+        )
+
+    def landed(layer, o):
+        owner = chunk_rows(at_offset(-o))
+        slot = lax.rem(o + n_tp, n_tp)
+        return pltpu.make_async_remote_copy(
+            src_ref=x_buf.at[layer + 1, owner],
+            dst_ref=x_buf.at[layer + 1, owner],
+            send_sem=x_send_sem.at[layer, slot],
+            recv_sem=x_recv_sem.at[layer, slot],
+            device_id={"tp": at_offset(1)},
+            device_id_type=MESH,
+        )
+
 
     loads["x"].wait()
     loads["norm"].wait()
@@ -246,7 +299,7 @@
     )
     for name in ("decay", "state", "rate", "freq", "b", "c", "feed", "w_out"):
         loads[name].wait()
-    pl.semaphore_wait(barrier, len(dp_steps) + len(tp_steps))
+    pl.semaphore_wait(barrier, len(dp_steps) + len(tp_greeted))
     for step in dp_steps:
         send_part(0, dp_peer(step))
     for layer in range(layers):
@@ -298,32 +351,24 @@
                 device_id_type=MESH,
             ).start()
 
-        for step in [(0, 0)] + dp_steps:
+        for step in dp_steps:
             s = dp_peer(step)
-            if step != (0, 0):
-                pltpu.make_async_remote_copy(
-                    src_ref=z_buf.at[layer, s],
-                    dst_ref=z_buf.at[layer, s],
-                    send_sem=z_send_sem.at[layer, s],
-                    recv_sem=z_recv_sem.at[layer, s],
-                    device_id={"dp": s},
-                    device_id_type=MESH,
-                ).wait_recv()
-            terms = jnp.dot(z_buf[layer, s], w_out[layer], preferred_element_type=F32)
-            for k in range(per_block):
-                t = s * per_block + k
-                term_buf[layer, t] = terms[k * chunk : (k + 1) * chunk].astype(BF16)
-
-                @pl.when(t != j)
-                def _():
-                    pltpu.make_async_remote_copy(
-                        src_ref=term_buf.at[layer, t],
-                        dst_ref=term_recv.at[layer, j],
-                        send_sem=term_send_sem.at[layer, t],
-                        recv_sem=term_recv_sem.at[layer, j],
-                        device_id={"tp": t},
-                        device_id_type=MESH,
-                    ).start()
+            pltpu.make_async_remote_copy(
+                src_ref=z_buf.at[layer, s],
+                dst_ref=z_buf.at[layer, s],
+                send_sem=z_send_sem.at[layer, s],
+                recv_sem=z_recv_sem.at[layer, s],
+                device_id={"dp": s},
+                device_id_type=MESH,
+            ).wait_recv()
+        terms = jnp.dot(
+            z_buf[layer].reshape(rows, chans), w_out[layer], preferred_element_type=F32
+        )
+        term_buf[layer] = terms.astype(BF16).reshape(n_tp, chunk, local_d)
+
+        up(layer, far).start()
+        for o in leaves:
+            up(layer, o).start()
 
         spread = jnp.where(own_group[None], u_f[:, None, :], 0.0).astype(BF16)
         spread = spread.reshape(mine * groups, chans)
@@ -333,42 +378,33 @@
         carried[layer] = carried[layer] + driven.reshape(mine, groups, width)
         pltpu.make_async_copy(carried.at[layer], state_out.at[layer], out_sem.at[layer]).start()
 
+        arrived(layer, far).wait_recv()
+        for o in hubs:
+            owner = at_offset(-o)
+            total = term_buf[layer, owner].astype(F32)
+            for c in children[o]:
+                arrived(layer, c).wait_recv()
+                total = total + term_recv[layer, c % n_tp].astype(F32)
+            if abs(o) == hub:
+                last = term_recv[layer, far].astype(F32)
+                total = total + jnp.where(side * o > 0, last, 0.0)
+            term_buf[layer, owner] = total.astype(BF16)
+            up(layer, o).start()
         total = term_buf[layer, j].astype(F32)
-        for step in tp_steps:
-            t = tp_peer(step)
-            pltpu.make_async_remote_copy(
-                src_ref=term_buf.at[layer, t],
-                dst_ref=term_recv.at[layer, t],
-                send_sem=term_send_sem.at[layer, t],
-                recv_sem=term_recv_sem.at[layer, t],
-                device_id={"tp": t},
-                device_id_type=MESH,
-            ).wait_recv()
-            total = total + term_recv[layer, t].astype(F32)
-        at = pl.ds(pl.multiple_of(j * chunk, chunk), chunk)
+        for o in sorted(children[0], key=abs):
+            arrived(layer, o).wait_recv()
+            total = total + term_recv[layer, o % n_tp].astype(F32)
+        at = chunk_rows(j)
         branch = total.astype(BF16).astype(F32)
         x_buf[layer + 1, at, :] = (x_buf[layer, at, :].astype(F32) + branch).astype(BF16)
-        for step in tp_steps:
-            t = tp_peer(step)
-            pltpu.make_async_remote_copy(
-                src_ref=x_buf.at[layer + 1, at],
-                dst_ref=x_buf.at[layer + 1, at],
-                send_sem=x_send_sem.at[layer, t],
-                recv_sem=x_recv_sem.at[layer, j],
-                device_id={"tp": t},
-                device_id_type=MESH,
-            ).start()
-
-        def await_chunk(t):
-            piece = pl.ds(pl.multiple_of(t * chunk, chunk), chunk)
-            pltpu.make_async_remote_copy(
-                src_ref=x_buf.at[layer + 1, piece],
-                dst_ref=x_buf.at[layer + 1, piece],
-                send_sem=x_send_sem.at[layer, t],
-                recv_sem=x_recv_sem.at[layer, t],
-                device_id={"tp": t},
-                device_id_type=MESH,
-            ).wait_recv()
+
+        for c in sorted(children[0], key=lambda o: -abs(o)):
+            down(layer, 0, c).start()
+        for o in sorted(hubs, key=abs):
+            landed(layer, o).wait_recv()
+            for c in children[o]:
+                down(layer, o, c).start()
+        down(layer, hub * side, far * side).start()
 
         if layer + 1 < layers:
             order = [0]
@@ -380,10 +416,11 @@
                 s = lax.rem(lax.div(j, per_block) + d, n_dp)
                 for k in range(per_block):
                     t = s * per_block + k
-                    if d == 0:
-                        pl.when(t != j)(functools.partial(await_chunk, t))
-                    else:
-                        await_chunk(t)
+                    o = lax.rem(j - t + n_tp, n_tp)
+                    ready = o != 0
+                    for h in hubs:
+                        ready = ready & (o != h % n_tp)
+                    pl.when(ready)(lambda o=o: landed(layer, o).wait_recv())
                 piece = pl.ds(pl.multiple_of(s * mine, mine), mine)
                 x = x_buf[layer + 1, piece, :].astype(F32)
                 scaled = (x * norm[layer + 1 : layer + 2, :]).astype(BF16)
@@ -393,8 +430,8 @@
                 ).astype(BF16)
                 pl.when(s != i)(functools.partial(send_part, layer + 1, s))
         else:
-            for step in tp_steps:
-                await_chunk(tp_peer(step))
+            for o in [*leaves, far]:
+                landed(layer, o).wait_recv()
             pltpu.make_async_copy(x_buf.at[layers], tokens_out, out_sem.at[layers]).start()
 
     for layer in range(layers):
@@ -420,25 +457,11 @@
                 device_id={"dp": s},
                 device_id_type=MESH,
             ).wait_send()
-        for step in tp_steps:
-            t = tp_peer(step)
-            pltpu.make_async_remote_copy(
-                src_ref=term_buf.at[layer, t],
-                dst_ref=term_recv.at[layer, j],
-                send_sem=term_send_sem.at[layer, t],
-                recv_sem=term_recv_sem.at[layer, j],
-                device_id={"tp": t},
-                device_id_type=MESH,
-            ).wait_send()
-            at = pl.ds(pl.multiple_of(j * chunk, chunk), chunk)
-            pltpu.make_async_remote_copy(
-                src_ref=x_buf.at[layer + 1, at],
-                dst_ref=x_buf.at[layer + 1, at],
-                send_sem=x_send_sem.at[layer, t],
-                recv_sem=x_recv_sem.at[layer, j],
-                device_id={"tp": t},
-                device_id_type=MESH,
-            ).wait_send()
+        for o in [*tree, far]:
+            up(layer, o).wait_send()
+        for o in tree:
+            down(layer, tree[o], o).wait_send()
+        down(layer, hub * side, far * side).wait_send()
         pltpu.make_async_copy(carried.at[layer], state_out.at[layer], out_sem.at[layer]).wait()
     pltpu.make_async_copy(x_buf.at[layers], tokens_out, out_sem.at[layers]).wait()
 

time: 114 us -> 92.7 us (0.81)
  the two profiles are of different devices: /device:TPU:39 before, /device:TPU:40 now
where the time goes in v2:
time: 92.7 us; the launch traced here: 92.6 us
  Pallas kernels  89.5 us (97%)
  local copies, waits for them, and re-layouts  2.42 us (3%)
    pallas_call x1, Pallas kernels, on_device(): pl.pallas_call(functools.partial(kernel, n_dp, n_tp, n_dp * local_d), out...  89.5 us
    unnamed x4, local copies, waits for them, and re-layouts  2.42 us

profile of v2, /device:TPU:40, one launch (start us, length us, event | category | flops | bytes accessed | tf_op | source)
XLA Modules:
  0.0 92.6 jit_solution(4905011477427268630)
XLA Ops:
  0.6 89.5 %shard_map.149 = (bf16[256,512]{1,0:T(8,128)(2,1)}, f32[2,32,8,128]{3,2,1,0:T(8,128)}) custom-call(s32[32]{0:T(128)} %lengths.1, f32[2,8]{1,0:T(2,128)} %step_width.1, bf16[256,512]{1,0:T(8,128)(2,1)} %tokens_hbm.1, f32[2,512]{1,0:T(2,128)} %norm_hbm.1, bf16[2,512,128]{2,1,0:T(8,128)(2,1)} %w_in_hbm.1, bf16[2,512,128]{2,1,0:T(8,128)(2,1)} %w_gate_hbm.1, ...), custom_call_target="tpu_custom_call" | custom-call | tf_op jit(solution)/shard_map/pallas_call | solution.py:533
  90.1 0.0 copy-start
  90.1 1.7 %copy.18 = bf16[256,512]{1,0:T(8,128)(2,1)} copy(bf16[256,512]{1,0:T(8,128)(2,1)} %get-tuple-element.4) | data formatting | bytes 524288
  91.9 0.0 copy-done
  91.9 0.7 copy.19
Async XLA Ops:
  90.1 1.7 %copy-start = (f32[2,32,8,128]{3,2,1,0:T(8,128)S(1)}, f32[2,32,8,128]{3,2,1,0:T(8,128)}, u32[]{:S(2)}) copy-start(f32[2,32,8,128]{3,2,1,0:T(8,128)} %get-tuple-element.5) | copy-start | bytes 786436

commit v3 on v2

--- a/solution.py
+++ b/solution.py
@@ -45,8 +45,8 @@
     n_dp,
     n_tp,
     features,
-    lengths,
-    step_width,
+    lengths_hbm,
+    step_hbm,
     tokens_hbm,
     norm_hbm,
     w_in_hbm,
@@ -61,6 +61,8 @@
     w_out_hbm,
     tokens_out,
     state_out,
+    lengths,
+    step_width,
     x_buf,
     norm,
     w_cat,
@@ -128,13 +130,6 @@
     def at_offset(o):
         return lax.rem(j + o + n_tp, n_tp)
 
-    barrier = pltpu.get_barrier_semaphore()
-    for step in dp_steps:
-        pl.semaphore_signal(barrier, inc=1, device_id={"dp": dp_peer(step)}, device_id_type=MESH)
-    tp_greeted = sorted({(o - tree[o]) % n_tp for o in tree} | {2, n_tp - 2})
-    for step in tp_greeted:
-        pl.semaphore_signal(barrier, inc=1, device_id={"tp": at_offset(step)}, device_id_type=MESH)
-
     loads = {}
     for n, (name, src, dst) in enumerate(
         [
@@ -149,10 +144,24 @@
             ("b", b_hbm, b_mat),
             ("c", c_hbm, c_mat),
             ("feed", feed_hbm, feed),
+            ("lengths", lengths_hbm, lengths),
+            ("step", step_hbm, step_width),
             ("w_out", w_out_hbm, w_out),
         ]
     ):
         loads[name] = pltpu.make_async_copy(src, dst, local_sem.at[n])
+    for name in ("x", "norm", "w_in", "w_gate"):
+        loads[name].start()
+
+    barrier = pltpu.get_barrier_semaphore()
+    for step in dp_steps:
+        pl.semaphore_signal(barrier, inc=1, device_id={"dp": dp_peer(step)}, device_id_type=MESH)
+    tp_greeted = sorted({(o - tree[o]) % n_tp for o in tree} | {2, n_tp - 2})
+    for step in tp_greeted:
+        pl.semaphore_signal(barrier, inc=1, device_id={"tp": at_offset(step)}, device_id_type=MESH)
+
+    later = [name for name in loads if name not in ("x", "norm", "w_in", "w_gate")]
+    for name in later:
         loads[name].start()
 
     lane = lax.broadcasted_iota(jnp.int32, (groups, width), 1)
@@ -289,7 +298,7 @@
     scaled = (x * norm[0:1, :]).astype(BF16)
     squares = square_rows(x)
     for s in range(n_dp):
-        sq_buf[0, s, :, pl.ds(0, mine)] = squares[:, s * mine : (s + 1) * mine]
+        sq_buf[0, s, :, pl.ds(0, mine)] = squares[0:1, s * mine : (s + 1) * mine]
     loads["w_in"].wait()
     loads["w_gate"].wait()
     part_buf[0] = (
@@ -297,11 +306,11 @@
         .astype(BF16)
         .reshape(n_dp, mine, 2 * chans)
     )
-    for name in ("decay", "state", "rate", "freq", "b", "c", "feed", "w_out"):
-        loads[name].wait()
     pl.semaphore_wait(barrier, len(dp_steps) + len(tp_greeted))
     for step in dp_steps:
         send_part(0, dp_peer(step))
+    for name in later:
+        loads[name].wait()
     for layer in range(layers):
         prepare(layer)
 
@@ -375,8 +384,7 @@
         driven = jnp.dot(spread, drive_high[layer], preferred_element_type=F32) + jnp.dot(
             spread, drive_low[layer], preferred_element_type=F32
         )
-        carried[layer] = carried[layer] + driven.reshape(mine, groups, width)
-        pltpu.make_async_copy(carried.at[layer], state_out.at[layer], out_sem.at[layer]).start()
+        state_out[layer] = carried[layer] + driven.reshape(mine, groups, width)
 
         arrived(layer, far).wait_recv()
         for o in hubs:
@@ -424,7 +432,7 @@
                 piece = pl.ds(pl.multiple_of(s * mine, mine), mine)
                 x = x_buf[layer + 1, piece, :].astype(F32)
                 scaled = (x * norm[layer + 1 : layer + 2, :]).astype(BF16)
-                sq_buf[layer + 1, s, :, pl.ds(0, mine)] = square_rows(x)
+                sq_buf[layer + 1, s, :, pl.ds(0, mine)] = square_rows(x)[0:1]
                 part_buf[layer + 1, s] = jnp.dot(
                     scaled, w_cat[layer + 1], preferred_element_type=F32
                 ).astype(BF16)
@@ -432,7 +440,7 @@
         else:
             for o in [*leaves, far]:
                 landed(layer, o).wait_recv()
-            pltpu.make_async_copy(x_buf.at[layers], tokens_out, out_sem.at[layers]).start()
+            tokens_out[...] = x_buf[layers]
 
     for layer in range(layers):
         for step in dp_steps:
@@ -462,8 +470,6 @@
         for o in tree:
             down(layer, tree[o], o).wait_send()
         down(layer, hub * side, far * side).wait_send()
-        pltpu.make_async_copy(carried.at[layer], state_out.at[layer], out_sem.at[layer]).wait()
-    pltpu.make_async_copy(x_buf.at[layers], tokens_out, out_sem.at[layers]).wait()
 
 
 def on_device(
@@ -488,11 +494,13 @@
     rows, local_d = tokens.shape
     chans = output_weight.shape[1]
     chunk = rows // n_tp
-    smem = pl.BlockSpec(memory_space=pltpu.SMEM)
-    hbm = pl.BlockSpec(memory_space=pl.ANY)
+    hbm = pl.BlockSpec(memory_space=pltpu.HBM)
     dma = pltpu.SemaphoreType.DMA
+    in_hbm = lambda a: pltpu.with_memory_space_constraint(a, pltpu.HBM)
     like = lambda a: pltpu.VMEM(a.shape, a.dtype)
     scratch = [
+        pltpu.SMEM(sequence_lengths.shape, sequence_lengths.dtype),
+        pltpu.SMEM(discrete_step.shape, discrete_step.dtype),
         pltpu.VMEM((layers + 1, rows, local_d), BF16),
         like(norm_weight),
         pltpu.VMEM((layers, local_d, 2 * chans), BF16),
@@ -504,14 +512,14 @@
         like(group_input_matrix),
         like(group_output_matrix),
         like(feedthrough_weight),
-        dma((12,)),
+        dma((14,)),
         dma((layers + 1,)),
         pltpu.VMEM((layers, n_dp, mine, 2 * chans), BF16),
         pltpu.VMEM((layers, n_dp, mine, 2 * chans), BF16),
         dma((layers, n_dp)),
         dma((layers, n_dp)),
-        pltpu.VMEM((layers, n_dp, 8, 128), F32),
-        pltpu.VMEM((layers, n_dp, 8, 128), F32),
+        pltpu.VMEM((layers, n_dp, 1, 128), F32),
+        pltpu.VMEM((layers, n_dp, 1, 128), F32),
         dma((layers, n_dp)),
         dma((layers, n_dp)),
         pltpu.VMEM((layers, n_dp, mine, chans), BF16),
@@ -536,25 +544,25 @@
             jax.ShapeDtypeStruct(tokens.shape, tokens.dtype),
             jax.ShapeDtypeStruct(recurrent_state.shape, recurrent_state.dtype),
         ),
-        in_specs=[smem, smem] + [hbm] * 12,
-        out_specs=(hbm, hbm),
+        in_specs=[hbm] * 14,
+        out_specs=(pl.BlockSpec(memory_space=pltpu.VMEM),) * 2,
         scratch_shapes=scratch,
-        compiler_params=pltpu.CompilerParams(collective_id=0, has_side_effects=True),
+        compiler_params=pltpu.CompilerParams(collective_id=0, has_side_effects=True, vmem_limit_bytes=16 * 2**20),
     )(
-        sequence_lengths,
-        discrete_step,
-        tokens,
-        norm_weight,
-        input_weight,
-        gate_weight,
-        extra_log_decay,
-        recurrent_state,
-        negated_real_rate,
-        frequency,
-        group_input_matrix,
-        group_output_matrix,
-        feedthrough_weight,
-        output_weight,
+        in_hbm(sequence_lengths),
+        in_hbm(discrete_step),
+        in_hbm(tokens),
+        in_hbm(norm_weight),
+        in_hbm(input_weight),
+        in_hbm(gate_weight),
+        in_hbm(extra_log_decay),
+        in_hbm(recurrent_state),
+        in_hbm(negated_real_rate),
+        in_hbm(frequency),
+        in_hbm(group_input_matrix),
+        in_hbm(group_output_matrix),
+        in_hbm(feedthrough_weight),
+        in_hbm(output_weight),
     )
 
 

time: 92.7 us -> 89.1 us (0.961)
  Pallas kernels: 89.5 us -> 86.9 us
  local copies, waits for them, and re-layouts: 2.42 us -> 1.41 us
    pallas_call x1, Pallas kernels: 89.5 us -> 86.9 us  [on_device(): pl.pallas_call(functools.partial(kernel, n_dp, n_tp, n_dp * local_d), out...]
    unnamed x4 -> x2, local copies, waits for them, and re-layouts: 2.42 us -> 1.41 us
where the time goes in v3:
time: 89.1 us; the launch traced here: 89 us
  Pallas kernels  86.9 us (98%)
  local copies, waits for them, and re-layouts  1.41 us (2%)
    pallas_call x1, Pallas kernels, on_device(): pl.pallas_call(functools.partial(kernel, n_dp, n_tp, n_dp * local_d), out...  86.9 us

profile of v3, /device:TPU:40, one launch (start us, length us, event | category | flops | bytes accessed | tf_op | source)
XLA Modules:
  0.0 89.0 jit_solution(8200339982416458378)
XLA Ops:
  0.6 86.9 %shard_map.149 = (bf16[256,512]{1,0:T(8,128)(2,1)S(1)}, f32[2,32,8,128]{3,2,1,0:T(8,128)S(1)}) custom-call(s32[32]{0:T(128)} %lengths_hbm.1, f32[2,8]{1,0:T(2,128)} %step_hbm.1, bf16[256,512]{1,0:T(8,128)(2,1)} %tokens_hbm.1, f32[2,512]{1,0:T(2,128)} %norm_hbm.1, bf16[2,512,128]{2,1,0:T(8,128)(2,1)} %w_in_hbm.1, bf16[2,512,128]{2,1,0:T(8,128)(2,1)} %w_gate_hbm.1, ...), custom_call_target="tpu_custom_call" | custom-call | tf_op jit(solution)/shard_map/pallas_call | solution.py:541
  87.6 0.7 copy.18
  88.3 0.7 copy.19

commit v4 on v3

--- a/solution.py
+++ b/solution.py
@@ -99,6 +99,7 @@
     drive_low,
     mix_cat,
     base,
+    relay,
 ):
     i = lax.axis_index("dp")
     j = lax.axis_index("tp")
@@ -111,7 +112,7 @@
     channel_group = chans // groups
 
     dp_steps = [(0, 1)] + [
-        (d, e) for d in (1, n_dp // 2 - 1, 2) for e in (0, 1)
+        (d, e) for d in (1, n_dp // 2 - 1, n_dp // 4) for e in (0, 1)
     ]
 
     def dp_peer(step):
@@ -156,7 +157,7 @@
     barrier = pltpu.get_barrier_semaphore()
     for step in dp_steps:
         pl.semaphore_signal(barrier, inc=1, device_id={"dp": dp_peer(step)}, device_id_type=MESH)
-    tp_greeted = sorted({(o - tree[o]) % n_tp for o in tree} | {2, n_tp - 2})
+    tp_greeted = [o for o in (-3, 3, -2, 2, -1, 1)]
     for step in tp_greeted:
         pl.semaphore_signal(barrier, inc=1, device_id={"tp": at_offset(step)}, device_id_type=MESH)
 
@@ -241,6 +242,35 @@
                 device_id_type=MESH,
             ).start()
 
+    def await_sends(layer):
+        for step in dp_steps:
+            s = dp_peer(step)
+            for src, dst, ssem, rsem in (
+                (part_buf, part_recv, part_send_sem, part_recv_sem),
+                (sq_buf, sq_recv, sq_send_sem, sq_recv_sem),
+            ):
+                pltpu.make_async_remote_copy(
+                    src_ref=src.at[layer, s],
+                    dst_ref=dst.at[layer, i],
+                    send_sem=ssem.at[layer, s],
+                    recv_sem=rsem.at[layer, i],
+                    device_id={"dp": s},
+                    device_id_type=MESH,
+                ).wait_send()
+            pltpu.make_async_remote_copy(
+                src_ref=z_buf.at[layer, i],
+                dst_ref=z_buf.at[layer, i],
+                send_sem=z_send_sem.at[layer, s],
+                recv_sem=z_recv_sem.at[layer, i],
+                device_id={"dp": s},
+                device_id_type=MESH,
+            ).wait_send()
+        for o in [*tree, far]:
+            up(layer, o).wait_send()
+        for o in tree:
+            down(layer, tree[o], o).wait_send()
+        down(layer, hub * side, far * side).wait_send()
+
     ones = jnp.ones((8, 128), F32)
 
     def square_rows(x):
@@ -266,6 +296,17 @@
         )
 
     arrived = up
+
+    def climb(layer, owner, o, past, reach):
+        hop = (1 - 2 * past) * (reach - lax.div(reach + 1, 3) * 3)
+        pltpu.make_async_remote_copy(
+            src_ref=term_buf.at[layer, owner],
+            dst_ref=term_recv.at[layer, o],
+            send_sem=term_send_sem.at[layer, o],
+            recv_sem=term_recv_sem.at[layer, o],
+            device_id={"tp": at_offset(-hop)},
+            device_id_type=MESH,
+        ).start()
 
     def down(layer, o, c):
         owner = chunk_rows(at_offset(-o))
@@ -307,7 +348,9 @@
         .reshape(n_dp, mine, 2 * chans)
     )
     pl.semaphore_wait(barrier, len(dp_steps) + len(tp_greeted))
-    for step in dp_steps:
+    for step in (-hub // 2, hub // 2):
+        pl.semaphore_signal(relay, inc=1, device_id={"tp": at_offset(step)}, device_id_type=MESH)
+    for step in reversed(dp_steps):
         send_part(0, dp_peer(step))
     for name in later:
         loads[name].wait()
@@ -349,7 +392,7 @@
         )
         y = jax.nn.gelu(read + feed[layer : layer + 1, :] * u_f)
         z_buf[layer, i] = (y * jax.nn.sigmoid(gate)).astype(BF16)
-        for step in dp_steps:
+        for step in reversed(dp_steps):
             s = dp_peer(step)
             pltpu.make_async_remote_copy(
                 src_ref=z_buf.at[layer, i],
@@ -360,24 +403,30 @@
                 device_id_type=MESH,
             ).start()
 
-        for step in dp_steps:
+        for step in [(0, 0), *dp_steps]:
             s = dp_peer(step)
-            pltpu.make_async_remote_copy(
-                src_ref=z_buf.at[layer, s],
-                dst_ref=z_buf.at[layer, s],
-                send_sem=z_send_sem.at[layer, s],
-                recv_sem=z_recv_sem.at[layer, s],
-                device_id={"dp": s},
-                device_id_type=MESH,
-            ).wait_recv()
-        terms = jnp.dot(
-            z_buf[layer].reshape(rows, chans), w_out[layer], preferred_element_type=F32
-        )
-        term_buf[layer] = terms.astype(BF16).reshape(n_tp, chunk, local_d)
-
-        up(layer, far).start()
-        for o in leaves:
-            up(layer, o).start()
+            if step != (0, 0):
+                pltpu.make_async_remote_copy(
+                    src_ref=z_buf.at[layer, s],
+                    dst_ref=z_buf.at[layer, s],
+                    send_sem=z_send_sem.at[layer, s],
+                    recv_sem=z_recv_sem.at[layer, s],
+                    device_id={"dp": s},
+                    device_id_type=MESH,
+                ).wait_recv()
+            terms = jnp.dot(z_buf[layer, s], w_out[layer], preferred_element_type=F32)
+            for k in range(per_block):
+                owner = s * per_block + k
+                term_buf[layer, owner] = terms[k * chunk : (k + 1) * chunk].astype(BF16)
+            for k in range(per_block):
+                owner = s * per_block + k
+                o = lax.rem(j - owner + n_tp, n_tp)
+                past = lax.div(o, far + 1)
+                reach = o + past * (n_tp - 2 * o)
+                pl.when((lax.rem(reach, 3) != 0) & (reach != far))(
+                    functools.partial(climb, layer, owner, o, past, reach)
+                )
+                pl.when(reach == far)(lambda: up(layer, far).start())
 
         spread = jnp.where(own_group[None], u_f[:, None, :], 0.0).astype(BF16)
         spread = spread.reshape(mine * groups, chans)
@@ -386,6 +435,10 @@
         )
         state_out[layer] = carried[layer] + driven.reshape(mine, groups, width)
 
+        if layer == 0:
+            pl.semaphore_wait(relay, 2)
+        else:
+            await_sends(layer - 1)
         arrived(layer, far).wait_recv()
         for o in hubs:
             owner = at_offset(-o)
@@ -410,7 +463,7 @@
             down(layer, 0, c).start()
         for o in sorted(hubs, key=abs):
             landed(layer, o).wait_recv()
-            for c in children[o]:
+            for c in sorted(children[o], key=lambda c: -abs(c)):
                 down(layer, o, c).start()
         down(layer, hub * side, far * side).start()
 
@@ -442,34 +495,7 @@
                 landed(layer, o).wait_recv()
             tokens_out[...] = x_buf[layers]
 
-    for layer in range(layers):
-        for step in dp_steps:
-            s = dp_peer(step)
-            for src, dst, ssem, rsem in (
-                (part_buf, part_recv, part_send_sem, part_recv_sem),
-                (sq_buf, sq_recv, sq_send_sem, sq_recv_sem),
-            ):
-                pltpu.make_async_remote_copy(
-                    src_ref=src.at[layer, s],
-                    dst_ref=dst.at[layer, i],
-                    send_sem=ssem.at[layer, s],
-                    recv_sem=rsem.at[layer, i],
-                    device_id={"dp": s},
-                    device_id_type=MESH,
-                ).wait_send()
-            pltpu.make_async_remote_copy(
-                src_ref=z_buf.at[layer, i],
-                dst_ref=z_buf.at[layer, i],
-                send_sem=z_send_sem.at[layer, s],
-                recv_sem=z_recv_sem.at[layer, i],
-                device_id={"dp": s},
-                device_id_type=MESH,
-            ).wait_send()
-        for o in [*tree, far]:
-            up(layer, o).wait_send()
-        for o in tree:
-            down(layer, tree[o], o).wait_send()
-        down(layer, hub * side, far * side).wait_send()
+    await_sends(layers - 1)
 
 
 def on_device(
@@ -537,6 +563,7 @@
         pltpu.VMEM((layers, chans, width), BF16),
         pltpu.VMEM((layers, 2 * chans, chans), BF16),
         pltpu.VMEM((layers, mine, chans), F32),
+        pltpu.SemaphoreType.REGULAR,
     ]
     return pl.pallas_call(
         functools.partial(kernel, n_dp, n_tp, n_dp * local_d),

time: 89.1 us -> 86.8 us (0.974)
  Pallas kernels: 86.9 us -> 84.3 us
    pallas_call x1, Pallas kernels: 86.9 us -> 84.3 us  [on_device(): pl.pallas_call(functools.partial(kernel, n_dp, n_tp, n_dp * local_d), out...]
where the time goes in v4:
time: 86.8 us; the launch traced here: 86.3 us
  Pallas kernels  84.3 us (97%)
  local copies, waits for them, and re-layouts  1.41 us (2%)
    pallas_call x1, Pallas kernels, on_device(): pl.pallas_call(functools.partial(kernel, n_dp, n_tp, n_dp * local_d), out...  84.3 us

profile of v4, /device:TPU:40, one launch (start us, length us, event | category | flops | bytes accessed | tf_op | source)
XLA Modules:
  0.0 86.3 jit_solution(17806528621597120466)
XLA Ops:
  0.6 84.3 %shard_map.149 = (bf16[256,512]{1,0:T(8,128)(2,1)S(1)}, f32[2,32,8,128]{3,2,1,0:T(8,128)S(1)}) custom-call(s32[32]{0:T(128)} %lengths_hbm.1, f32[2,8]{1,0:T(2,128)} %step_hbm.1, bf16[256,512]{1,0:T(8,128)(2,1)} %tokens_hbm.1, f32[2,512]{1,0:T(2,128)} %norm_hbm.1, bf16[2,512,128]{2,1,0:T(8,128)(2,1)} %w_in_hbm.1, bf16[2,512,128]{2,1,0:T(8,128)(2,1)} %w_gate_hbm.1, ...), custom_call_target="tpu_custom_call" | custom-call | tf_op jit(solution)/shard_map/pallas_call | solution.py:568
  84.9 0.7 copy.18
  85.6 0.7 copy.19

commit v5 on v4

--- a/solution.py
+++ b/solution.py
@@ -75,7 +75,6 @@
     c_mat,
     feed,
     local_sem,
-    out_sem,
     part_buf,
     part_recv,
     part_send_sem,
@@ -236,40 +235,21 @@
             pltpu.make_async_remote_copy(
                 src_ref=src.at[layer, s],
                 dst_ref=dst.at[layer, i],
-                send_sem=ssem.at[layer, s],
-                recv_sem=rsem.at[layer, i],
+                send_sem=ssem.at[0],
+                recv_sem=rsem.at[0],
                 device_id={"dp": s},
                 device_id_type=MESH,
             ).start()
 
-    def await_sends(layer):
-        for step in dp_steps:
-            s = dp_peer(step)
-            for src, dst, ssem, rsem in (
-                (part_buf, part_recv, part_send_sem, part_recv_sem),
-                (sq_buf, sq_recv, sq_send_sem, sq_recv_sem),
-            ):
-                pltpu.make_async_remote_copy(
-                    src_ref=src.at[layer, s],
-                    dst_ref=dst.at[layer, i],
-                    send_sem=ssem.at[layer, s],
-                    recv_sem=rsem.at[layer, i],
-                    device_id={"dp": s},
-                    device_id_type=MESH,
-                ).wait_send()
-            pltpu.make_async_remote_copy(
-                src_ref=z_buf.at[layer, i],
-                dst_ref=z_buf.at[layer, i],
-                send_sem=z_send_sem.at[layer, s],
-                recv_sem=z_recv_sem.at[layer, i],
-                device_id={"dp": s},
-                device_id_type=MESH,
-            ).wait_send()
-        for o in [*tree, far]:
-            up(layer, o).wait_send()
-        for o in tree:
-            down(layer, tree[o], o).wait_send()
-        down(layer, hub * side, far * side).wait_send()
+    def await_sends():
+        for buf, sem in (
+            (part_buf.at[:, pl.ds(0, n_dp - 1)], part_send_sem),
+            (sq_buf.at[:, pl.ds(0, n_dp - 1)], sq_send_sem),
+            (z_buf.at[:, pl.ds(0, n_dp - 1)], z_send_sem),
+            (term_buf.at[:, pl.ds(0, n_tp - 1)], term_send_sem),
+            (x_buf.at[pl.ds(0, layers), pl.ds(0, rows - chunk)], x_send_sem),
+        ):
+            pltpu.make_async_copy(buf, buf, sem.at[0]).wait()
 
     ones = jnp.ones((8, 128), F32)
 
@@ -289,8 +269,8 @@
         return pltpu.make_async_remote_copy(
             src_ref=term_buf.at[layer, owner],
             dst_ref=term_recv.at[layer, o % n_tp],
-            send_sem=term_send_sem.at[layer, o % n_tp],
-            recv_sem=term_recv_sem.at[layer, o % n_tp],
+            send_sem=term_send_sem.at[0],
+            recv_sem=term_recv_sem.at[o % n_tp],
             device_id={"tp": at_offset(-hop)},
             device_id_type=MESH,
         )
@@ -302,8 +282,8 @@
         pltpu.make_async_remote_copy(
             src_ref=term_buf.at[layer, owner],
             dst_ref=term_recv.at[layer, o],
-            send_sem=term_send_sem.at[layer, o],
-            recv_sem=term_recv_sem.at[layer, o],
+            send_sem=term_send_sem.at[0],
+            recv_sem=term_recv_sem.at[o],
             device_id={"tp": at_offset(-hop)},
             device_id_type=MESH,
         ).start()
@@ -314,8 +294,8 @@
         return pltpu.make_async_remote_copy(
             src_ref=x_buf.at[layer + 1, owner],
             dst_ref=x_buf.at[layer + 1, owner],
-            send_sem=x_send_sem.at[layer, slot],
-            recv_sem=x_recv_sem.at[layer, slot],
+            send_sem=x_send_sem.at[0],
+            recv_sem=x_recv_sem.at[slot],
             device_id={"tp": at_offset(c - o)},
             device_id_type=MESH,
         )
@@ -326,8 +306,8 @@
         return pltpu.make_async_remote_copy(
             src_ref=x_buf.at[layer + 1, owner],
             dst_ref=x_buf.at[layer + 1, owner],
-            send_sem=x_send_sem.at[layer, slot],
-            recv_sem=x_recv_sem.at[layer, slot],
+            send_sem=x_send_sem.at[0],
+            recv_sem=x_recv_sem.at[slot],
             device_id={"tp": at_offset(1)},
             device_id_type=MESH,
         )
@@ -361,22 +341,13 @@
     row_sub = lax.broadcasted_iota(jnp.int32, (mine, 128), 0)
 
     for layer in range(layers):
+        for buf, sem in ((part_recv, part_recv_sem), (sq_recv, sq_recv_sem)):
+            others = buf.at[layer, pl.ds(0, n_dp - 1)]
+            pltpu.make_async_copy(others, others, sem.at[0]).wait()
         total = part_buf[layer, i].astype(F32)
         sq = sq_buf[layer, i]
         for step in dp_steps:
             s = dp_peer(step)
-            for src, dst, ssem, rsem in (
-                (part_buf, part_recv, part_send_sem, part_recv_sem),
-                (sq_buf, sq_recv, sq_send_sem, sq_recv_sem),
-            ):
-                pltpu.make_async_remote_copy(
-                    src_ref=src.at[layer, s],
-                    dst_ref=dst.at[layer, s],
-                    send_sem=ssem.at[layer, s],
-                    recv_sem=rsem.at[layer, s],
-                    device_id={"dp": s},
-                    device_id_type=MESH,
-                ).wait_recv()
             total = total + part_recv[layer, s].astype(F32)
             sq = sq + sq_recv[layer, s]
         mean = jnp.sum(
@@ -397,8 +368,8 @@
             pltpu.make_async_remote_copy(
                 src_ref=z_buf.at[layer, i],
                 dst_ref=z_buf.at[layer, i],
-                send_sem=z_send_sem.at[layer, s],
-                recv_sem=z_recv_sem.at[layer, i],
+                send_sem=z_send_sem.at[0],
+                recv_sem=z_recv_sem.at[i],
                 device_id={"dp": s},
                 device_id_type=MESH,
             ).start()
@@ -409,8 +380,8 @@
                 pltpu.make_async_remote_copy(
                     src_ref=z_buf.at[layer, s],
                     dst_ref=z_buf.at[layer, s],
-                    send_sem=z_send_sem.at[layer, s],
-                    recv_sem=z_recv_sem.at[layer, s],
+                    send_sem=z_send_sem.at[0],
+                    recv_sem=z_recv_sem.at[s],
                     device_id={"dp": s},
                     device_id_type=MESH,
                 ).wait_recv()
@@ -437,8 +408,6 @@
 
         if layer == 0:
             pl.semaphore_wait(relay, 2)
-        else:
-            await_sends(layer - 1)
         arrived(layer, far).wait_recv()
         for o in hubs:
             owner = at_offset(-o)
@@ -495,7 +464,7 @@
                 landed(layer, o).wait_recv()
             tokens_out[...] = x_buf[layers]
 
-    await_sends(layers - 1)
+    await_sends()
 
 
 def on_device(
@@ -539,24 +508,23 @@
         like(group_output_matrix),
         like(feedthrough_weight),
         dma((14,)),
-        dma((layers + 1,)),
         pltpu.VMEM((layers, n_dp, mine, 2 * chans), BF16),
         pltpu.VMEM((layers, n_dp, mine, 2 * chans), BF16),
-        dma((layers, n_dp)),
-        dma((layers, n_dp)),
+        dma((1,)),
+        dma((1,)),
         pltpu.VMEM((layers, n_dp, 1, 128), F32),
         pltpu.VMEM((layers, n_dp, 1, 128), F32),
-        dma((layers, n_dp)),
-        dma((layers, n_dp)),
+        dma((1,)),
+        dma((1,)),
         pltpu.VMEM((layers, n_dp, mine, chans), BF16),
-        dma((layers, n_dp)),
-        dma((layers, n_dp)),
+        dma((1,)),
+        dma((n_dp,)),
         pltpu.VMEM((layers, n_tp, chunk, local_d), BF16),
         pltpu.VMEM((layers, n_tp, chunk, local_d), BF16),
-        dma((layers, n_tp)),
-        dma((layers, n_tp)),
-        dma((layers, n_tp)),
-        dma((layers, n_tp)),
+        dma((1,)),
+        dma((n_tp,)),
+        dma((1,)),
+        dma((n_tp,)),
         pltpu.VMEM((mine, groups, width), F32),
         pltpu.VMEM((layers, mine, groups, width), F32),
         pltpu.VMEM((layers, chans, width), BF16),

time: 86.8 us -> 84.8 us (0.977)
  Pallas kernels: 84.3 us -> 82.7 us
    pallas_call x1, Pallas kernels: 84.3 us -> 82.7 us  [on_device(): pl.pallas_call(functools.partial(kernel, n_dp, n_tp, n_dp * local_d), out...]
where the time goes in v5:
time: 84.8 us; the launch traced here: 84.7 us
  Pallas kernels  82.7 us (98%)
  local copies, waits for them, and re-layouts  1.41 us (2%)
    pallas_call x1, Pallas kernels, on_device(): pl.pallas_call(functools.partial(kernel, n_dp, n_tp, n_dp * local_d), out...  82.7 us

profile of v5, /device:TPU:40, one launch (start us, length us, event | category | flops | bytes accessed | tf_op | source)
XLA Modules:
  0.0 84.7 jit_solution(15126996298892282931)
XLA Ops:
  0.6 82.7 %shard_map.149 = (bf16[256,512]{1,0:T(8,128)(2,1)S(1)}, f32[2,32,8,128]{3,2,1,0:T(8,128)S(1)}) custom-call(s32[32]{0:T(128)} %lengths_hbm.1, f32[2,8]{1,0:T(2,128)} %step_hbm.1, bf16[256,512]{1,0:T(8,128)(2,1)} %tokens_hbm.1, f32[2,512]{1,0:T(2,128)} %norm_hbm.1, bf16[2,512,128]{2,1,0:T(8,128)(2,1)} %w_in_hbm.1, bf16[2,512,128]{2,1,0:T(8,128)(2,1)} %w_gate_hbm.1, ...), custom_call_target="tpu_custom_call" | custom-call | tf_op jit(solution)/shard_map/pallas_call | solution.py:536
  83.3 0.7 copy.18
  84.0 0.7 copy.19

commit v6 on v5

--- a/solution.py
+++ b/solution.py
@@ -104,10 +104,10 @@
     j = lax.axis_index("tp")
     layers, mine, groups, width = state.shape
     half = width // 2
-    rows, local_d = x_buf.shape[1:]
+    halves, per_block, chunk, local_d = x_buf.shape[2:]
+    rows = n_dp * mine
+    part_rows = mine // halves
     chans = w_out.shape[1]
-    chunk = rows // n_tp
-    per_block = mine // chunk
     channel_group = chans // groups
 
     dp_steps = [(0, 1)] + [
@@ -127,6 +127,11 @@
     leaves = [o for o in by_reach if not children[o]]
     hubs = [o for o in by_reach if children[o]]
 
+    near_hub = [c for o in hubs if abs(o) != hub for c in children[o]]
+    far_hub = [c for o in hubs if abs(o) == hub for c in children[o]] + [far]
+    up_group = {o: 0 if o in far_hub else 1 if o in near_hub else 2 for o in [*tree, far]}
+    down_group = {o: 1 + hubs.index(o) if o in hubs else 0 for o in [*tree, far]}
+
     def at_offset(o):
         return lax.rem(j + o + n_tp, n_tp)
 
@@ -135,8 +140,10 @@
         [
             ("x", tokens_hbm, x_buf.at[0]),
             ("norm", norm_hbm, norm),
-            ("w_in", w_in_hbm, w_cat.at[:, :, pl.ds(0, chans)]),
-            ("w_gate", w_gate_hbm, w_cat.at[:, :, pl.ds(chans, chans)]),
+            ("w_in", w_in_hbm.at[0], w_cat.at[0, :, pl.ds(0, chans)]),
+            ("w_gate", w_gate_hbm.at[0], w_cat.at[0, :, pl.ds(chans, chans)]),
+            ("w_in_1", w_in_hbm.at[1], w_cat.at[1, :, pl.ds(0, chans)]),
+            ("w_gate_1", w_gate_hbm.at[1], w_cat.at[1, :, pl.ds(chans, chans)]),
             ("decay", decay_hbm, decay),
             ("state", state_hbm, state),
             ("rate", rate_hbm, rate),
@@ -227,27 +234,27 @@
         read = jnp.where(own_group[None], read.reshape(mine, groups, chans), 0.0)
         base[layer] = jnp.sum(read, axis=1)
 
-    def send_part(layer, s):
+    def send_part(layer, h, s):
         for src, dst, ssem, rsem in (
             (part_buf, part_recv, part_send_sem, part_recv_sem),
             (sq_buf, sq_recv, sq_send_sem, sq_recv_sem),
         ):
             pltpu.make_async_remote_copy(
-                src_ref=src.at[layer, s],
-                dst_ref=dst.at[layer, i],
+                src_ref=src.at[layer, h, s],
+                dst_ref=dst.at[layer, h, i],
                 send_sem=ssem.at[0],
-                recv_sem=rsem.at[0],
+                recv_sem=rsem.at[h],
                 device_id={"dp": s},
                 device_id_type=MESH,
             ).start()
 
     def await_sends():
         for buf, sem in (
-            (part_buf.at[:, pl.ds(0, n_dp - 1)], part_send_sem),
-            (sq_buf.at[:, pl.ds(0, n_dp - 1)], sq_send_sem),
-            (z_buf.at[:, pl.ds(0, n_dp - 1)], z_send_sem),
-            (term_buf.at[:, pl.ds(0, n_tp - 1)], term_send_sem),
-            (x_buf.at[pl.ds(0, layers), pl.ds(0, rows - chunk)], x_send_sem),
+            (part_buf.at[:, :, pl.ds(0, n_dp - 1)], part_send_sem),
+            (sq_buf.at[:, :, pl.ds(0, n_dp - 1)], sq_send_sem),
+            (z_buf.at[:, :, pl.ds(0, n_dp - 1)], z_send_sem),
+            (term_buf.at[:, :, pl.ds(0, n_tp - 1)], term_send_sem),
+            (term_buf.at[:, :, pl.ds(0, n_tp - 1)], x_send_sem),
         ):
             pltpu.make_async_copy(buf, buf, sem.at[0]).wait()
 
@@ -260,211 +267,240 @@
             total = total + x2[:, k * 128 : (k + 1) * 128]
         return contract_last(ones, total, HIGHEST)
 
-    def chunk_rows(t):
-        return pl.ds(pl.multiple_of(t * chunk, chunk), chunk)
-
-    def up(layer, o):
+    def of_owner(layer, h, t):
+        return x_buf.at[layer, lax.div(t, per_block), h, lax.rem(t, per_block)]
+
+    def up(layer, h, o):
         hop = 2 * side if o == far else o - tree[o]
         owner = at_offset(-o)
         return pltpu.make_async_remote_copy(
-            src_ref=term_buf.at[layer, owner],
-            dst_ref=term_recv.at[layer, o % n_tp],
+            src_ref=term_buf.at[layer, h, owner],
+            dst_ref=term_recv.at[layer, h, o % n_tp],
             send_sem=term_send_sem.at[0],
-            recv_sem=term_recv_sem.at[o % n_tp],
+            recv_sem=term_recv_sem.at[h, up_group[o]],
             device_id={"tp": at_offset(-hop)},
             device_id_type=MESH,
         )
 
-    arrived = up
-
-    def climb(layer, owner, o, past, reach):
+    def climb(layer, h, owner, o, past, reach):
         hop = (1 - 2 * past) * (reach - lax.div(reach + 1, 3) * 3)
         pltpu.make_async_remote_copy(
-            src_ref=term_buf.at[layer, owner],
-            dst_ref=term_recv.at[layer, o],
+            src_ref=term_buf.at[layer, h, owner],
+            dst_ref=term_recv.at[layer, h, o],
             send_sem=term_send_sem.at[0],
-            recv_sem=term_recv_sem.at[o],
+            recv_sem=term_recv_sem.at[h, 2 - lax.div(reach + 1, 3)],
             device_id={"tp": at_offset(-hop)},
             device_id_type=MESH,
         ).start()
 
-    def down(layer, o, c):
-        owner = chunk_rows(at_offset(-o))
-        slot = lax.rem(c + n_tp, n_tp)
+    def down(layer, h, o, c):
+        piece = of_owner(layer + 1, h, at_offset(-o))
         return pltpu.make_async_remote_copy(
-            src_ref=x_buf.at[layer + 1, owner],
-            dst_ref=x_buf.at[layer + 1, owner],
+            src_ref=piece,
+            dst_ref=piece,
             send_sem=x_send_sem.at[0],
-            recv_sem=x_recv_sem.at[slot],
+            recv_sem=x_recv_sem.at[h, down_group.get(c if isinstance(c, int) else far, 0)],
             device_id={"tp": at_offset(c - o)},
             device_id_type=MESH,
         )
 
-    def landed(layer, o):
-        owner = chunk_rows(at_offset(-o))
-        slot = lax.rem(o + n_tp, n_tp)
+    def await_copies(buf, count, sem):
+        some = buf.at[pl.ds(0, count)]
+        pltpu.make_async_copy(some, some, sem).wait()
+
+    def await_hub_chunk(layer, h, o):
+        await_copies(term_buf.at[layer, h], 1, x_recv_sem.at[h, down_group[o]])
+
+    def await_leaf_chunks(layer, h):
+        await_copies(term_buf.at[layer, h], len(leaves) + 1, x_recv_sem.at[h, 0])
+
+    def z_copy(layer, h, s, owner):
         return pltpu.make_async_remote_copy(
-            src_ref=x_buf.at[layer + 1, owner],
-            dst_ref=x_buf.at[layer + 1, owner],
-            send_sem=x_send_sem.at[0],
-            recv_sem=x_recv_sem.at[slot],
-            device_id={"tp": at_offset(1)},
+            src_ref=z_buf.at[layer, h, owner],
+            dst_ref=z_buf.at[layer, h, owner],
+            send_sem=z_send_sem.at[0],
+            recv_sem=z_recv_sem.at[owner if h == 0 else n_dp],
+            device_id={"dp": s},
             device_id_type=MESH,
         )
 
-
     loads["x"].wait()
     loads["norm"].wait()
-    x = x_buf[0].astype(F32)
+    x = x_buf[0].astype(F32).reshape(rows, local_d)
     scaled = (x * norm[0:1, :]).astype(BF16)
     squares = square_rows(x)
     for s in range(n_dp):
-        sq_buf[0, s, :, pl.ds(0, mine)] = squares[0:1, s * mine : (s + 1) * mine]
+        for h in range(halves):
+            at = s * mine + h * part_rows
+            sq_buf[0, h, s, :, pl.ds(0, part_rows)] = squares[0:1, at : at + part_rows]
     loads["w_in"].wait()
     loads["w_gate"].wait()
-    part_buf[0] = (
-        jnp.dot(scaled, w_cat[0], preferred_element_type=F32)
-        .astype(BF16)
-        .reshape(n_dp, mine, 2 * chans)
-    )
+    parts = jnp.dot(scaled, w_cat[0], preferred_element_type=F32).astype(BF16)
+    for s in range(n_dp):
+        for h in range(halves):
+            at = s * mine + h * part_rows
+            part_buf[0, h, s] = parts[at : at + part_rows]
     pl.semaphore_wait(barrier, len(dp_steps) + len(tp_greeted))
     for step in (-hub // 2, hub // 2):
         pl.semaphore_signal(relay, inc=1, device_id={"tp": at_offset(step)}, device_id_type=MESH)
-    for step in reversed(dp_steps):
-        send_part(0, dp_peer(step))
+    for h in range(halves):
+        for step in reversed(dp_steps):
+            send_part(0, h, dp_peer(step))
     for name in later:
         loads[name].wait()
     for layer in range(layers):
         prepare(layer)
 
-    row_lane = lax.broadcasted_iota(jnp.int32, (mine, 128), 1)
-    row_sub = lax.broadcasted_iota(jnp.int32, (mine, 128), 0)
-
-    for layer in range(layers):
+    row_lane = lax.broadcasted_iota(jnp.int32, (part_rows, 128), 1)
+    row_sub = lax.broadcasted_iota(jnp.int32, (part_rows, 128), 0)
+
+    def mix(layer, h):
         for buf, sem in ((part_recv, part_recv_sem), (sq_recv, sq_recv_sem)):
-            others = buf.at[layer, pl.ds(0, n_dp - 1)]
-            pltpu.make_async_copy(others, others, sem.at[0]).wait()
-        total = part_buf[layer, i].astype(F32)
-        sq = sq_buf[layer, i]
+            others = buf.at[layer, h, pl.ds(0, n_dp - 1)]
+            pltpu.make_async_copy(others, others, sem.at[h]).wait()
+        total = part_buf[layer, h, i].astype(F32)
+        sq = sq_buf[layer, h, i]
         for step in dp_steps:
             s = dp_peer(step)
-            total = total + part_recv[layer, s].astype(F32)
-            sq = sq + sq_recv[layer, s]
+            total = total + part_recv[layer, h, s].astype(F32)
+            sq = sq + sq_recv[layer, h, s]
         mean = jnp.sum(
             jnp.where(row_lane == row_sub, sq[0:1, :], 0.0), axis=1, keepdims=True
         ) / features
-        scale = lax.rsqrt(mean + NORM_EPS)
-        total = total * scale
+        total = total * lax.rsqrt(mean + NORM_EPS)
         u = total[:, :chans].astype(BF16)
         gate = total[:, chans:].astype(BF16).astype(F32)
         u_f = u.astype(F32)
-        read = base[layer] + jnp.dot(
+        read = base[layer, h * part_rows : (h + 1) * part_rows] + jnp.dot(
             jnp.concatenate([u, u], axis=1), mix_cat[layer], preferred_element_type=F32
         )
         y = jax.nn.gelu(read + feed[layer : layer + 1, :] * u_f)
-        z_buf[layer, i] = (y * jax.nn.sigmoid(gate)).astype(BF16)
+        z_buf[layer, h, i] = (y * jax.nn.sigmoid(gate)).astype(BF16)
         for step in reversed(dp_steps):
-            s = dp_peer(step)
-            pltpu.make_async_remote_copy(
-                src_ref=z_buf.at[layer, i],
-                dst_ref=z_buf.at[layer, i],
-                send_sem=z_send_sem.at[0],
-                recv_sem=z_recv_sem.at[i],
-                device_id={"dp": s},
-                device_id_type=MESH,
-            ).start()
-
+            z_copy(layer, h, dp_peer(step), i).start()
+        return u_f
+
+    def project_streamed(layer, h):
         for step in [(0, 0), *dp_steps]:
             s = dp_peer(step)
             if step != (0, 0):
-                pltpu.make_async_remote_copy(
-                    src_ref=z_buf.at[layer, s],
-                    dst_ref=z_buf.at[layer, s],
-                    send_sem=z_send_sem.at[0],
-                    recv_sem=z_recv_sem.at[s],
-                    device_id={"dp": s},
-                    device_id_type=MESH,
-                ).wait_recv()
-            terms = jnp.dot(z_buf[layer, s], w_out[layer], preferred_element_type=F32)
+                z_copy(layer, h, s, s).wait_recv()
+            terms = jnp.dot(z_buf[layer, h, s], w_out[layer], preferred_element_type=F32)
             for k in range(per_block):
                 owner = s * per_block + k
-                term_buf[layer, owner] = terms[k * chunk : (k + 1) * chunk].astype(BF16)
+                term_buf[layer, h, owner] = terms[k * chunk : (k + 1) * chunk].astype(BF16)
             for k in range(per_block):
                 owner = s * per_block + k
                 o = lax.rem(j - owner + n_tp, n_tp)
                 past = lax.div(o, far + 1)
                 reach = o + past * (n_tp - 2 * o)
                 pl.when((lax.rem(reach, 3) != 0) & (reach != far))(
-                    functools.partial(climb, layer, owner, o, past, reach)
+                    functools.partial(climb, layer, h, owner, o, past, reach)
                 )
-                pl.when(reach == far)(lambda: up(layer, far).start())
-
+                pl.when(reach == far)(lambda: up(layer, h, far).start())
+
+    def project_at_once(layer, h):
+        await_copies(z_buf.at[layer, h], n_dp - 1, z_recv_sem.at[n_dp])
+        z = z_buf[layer, h].reshape(n_dp * part_rows, chans)
+        terms = jnp.dot(z, w_out[layer], preferred_element_type=F32)
+        term_buf[layer, h] = terms.reshape(n_tp, chunk, local_d).astype(BF16)
+        up(layer, h, far).start()
+        for o in leaves:
+            up(layer, h, o).start()
+
+    def project(layer, h):
+        (project_streamed if h == 0 else project_at_once)(layer, h)
+
+    def new_state(layer, h, u_f):
+        at = pl.ds(h * part_rows, part_rows)
         spread = jnp.where(own_group[None], u_f[:, None, :], 0.0).astype(BF16)
-        spread = spread.reshape(mine * groups, chans)
+        spread = spread.reshape(part_rows * groups, chans)
         driven = jnp.dot(spread, drive_high[layer], preferred_element_type=F32) + jnp.dot(
             spread, drive_low[layer], preferred_element_type=F32
         )
-        state_out[layer] = carried[layer] + driven.reshape(mine, groups, width)
-
+        state_out[layer, at] = carried[layer, at] + driven.reshape(part_rows, groups, width)
+
+    def sum_at_hubs(layer, h):
+        for group, under in enumerate((far_hub, near_hub)):
+            await_copies(term_recv.at[layer, h], len(under), term_recv_sem.at[h, group])
+            for o in hubs:
+                if children[o][0] not in under:
+                    continue
+                owner = at_offset(-o)
+                total = term_buf[layer, h, owner].astype(F32)
+                for c in children[o]:
+                    total = total + term_recv[layer, h, c % n_tp].astype(F32)
+                if abs(o) == hub:
+                    last = term_recv[layer, h, far].astype(F32)
+                    total = total + jnp.where(side * o > 0, last, 0.0)
+                term_buf[layer, h, owner] = total.astype(BF16)
+                up(layer, h, o).start()
+
+    def own_chunk(layer, h):
+        total = term_buf[layer, h, j].astype(F32)
+        await_copies(term_recv.at[layer, h], len(children[0]), term_recv_sem.at[h, 2])
+        for o in sorted(children[0], key=abs):
+            total = total + term_recv[layer, h, o % n_tp].astype(F32)
+        branch = total.astype(BF16).astype(F32)
+        x = of_owner(layer, h, j)[...].astype(F32)
+        of_owner(layer + 1, h, j)[...] = (x + branch).astype(BF16)
+        for c in sorted(children[0], key=lambda o: -abs(o)):
+            down(layer, h, 0, c).start()
+
+    def hand_down(layer, h):
+        for o in sorted(hubs, key=abs):
+            await_hub_chunk(layer, h, o)
+            for c in sorted(children[o], key=lambda c: -abs(c)):
+                down(layer, h, o, c).start()
+        down(layer, h, hub * side, far * side).start()
+
+    def next_parts(layer, h):
+        await_leaf_chunks(layer, h)
+        x = x_buf[layer + 1, :, h].astype(F32).reshape(n_dp * part_rows, local_d)
+        scaled = (x * norm[layer + 1 : layer + 2, :]).astype(BF16)
+        parts = jnp.dot(scaled, w_cat[layer + 1], preferred_element_type=F32)
+        part_buf[layer + 1, h] = parts.reshape(n_dp, part_rows, 2 * chans).astype(BF16)
+        squares = square_rows(x)
+        for s in range(n_dp):
+            at = s * part_rows
+            sq_buf[layer + 1, h, s, :, pl.ds(0, part_rows)] = squares[0:1, at : at + part_rows]
+        for step in reversed(dp_steps):
+            send_part(layer + 1, h, dp_peer(step))
+
+    both = range(halves)
+    for layer in range(layers):
+        u_f = [mix(layer, h) for h in both]
+        for h in both:
+            project(layer, h)
+        for h in both:
+            new_state(layer, h, u_f[h])
         if layer == 0:
             pl.semaphore_wait(relay, 2)
-        arrived(layer, far).wait_recv()
-        for o in hubs:
-            owner = at_offset(-o)
-            total = term_buf[layer, owner].astype(F32)
-            for c in children[o]:
-                arrived(layer, c).wait_recv()
-                total = total + term_recv[layer, c % n_tp].astype(F32)
-            if abs(o) == hub:
-                last = term_recv[layer, far].astype(F32)
-                total = total + jnp.where(side * o > 0, last, 0.0)
-            term_buf[layer, owner] = total.astype(BF16)
-            up(layer, o).start()
-        total = term_buf[layer, j].astype(F32)
-        for o in sorted(children[0], key=abs):
-            arrived(layer, o).wait_recv()
-            total = total + term_recv[layer, o % n_tp].astype(F32)
-        at = chunk_rows(j)
-        branch = total.astype(BF16).astype(F32)
-        x_buf[layer + 1, at, :] = (x_buf[layer, at, :].astype(F32) + branch).astype(BF16)
-
-        for c in sorted(children[0], key=lambda o: -abs(o)):
-            down(layer, 0, c).start()
-        for o in sorted(hubs, key=abs):
-            landed(layer, o).wait_recv()
-            for c in sorted(children[o], key=lambda c: -abs(c)):
-                down(layer, o, c).start()
-        down(layer, hub * side, far * side).start()
-
+        for h in both:
+            sum_at_hubs(layer, h)
+        for h in both:
+            own_chunk(layer, h)
+        for h in both:
+            hand_down(layer, h)
         if layer + 1 < layers:
-            order = [0]
-            for d in range(1, n_dp // 2 + 1):
-                order.append(d)
-                if n_dp - d != d:
-                    order.append(n_dp - d)
-            for d in order:
-                s = lax.rem(lax.div(j, per_block) + d, n_dp)
-                for k in range(per_block):
-                    t = s * per_block + k
-                    o = lax.rem(j - t + n_tp, n_tp)
-                    ready = o != 0
-                    for h in hubs:
-                        ready = ready & (o != h % n_tp)
-                    pl.when(ready)(lambda o=o: landed(layer, o).wait_recv())
-                piece = pl.ds(pl.multiple_of(s * mine, mine), mine)
-                x = x_buf[layer + 1, piece, :].astype(F32)
-                scaled = (x * norm[layer + 1 : layer + 2, :]).astype(BF16)
-                sq_buf[layer + 1, s, :, pl.ds(0, mine)] = square_rows(x)[0:1]
-                part_buf[layer + 1, s] = jnp.dot(
-                    scaled, w_cat[layer + 1], preferred_element_type=F32
-                ).astype(BF16)
-                pl.when(s != i)(functools.partial(send_part, layer + 1, s))
-        else:
-            for o in [*leaves, far]:
-                landed(layer, o).wait_recv()
-            tokens_out[...] = x_buf[layers]
+            for h in both:
+                next_parts(layer, h)
+    for h in both:
+        await_leaf_chunks(layers - 1, h)
+        tokens_out[:, h] = x_buf[layers, :, h]
 
     await_sends()
+
+
+def write_out(tokens, state, tokens_out, state_out, sem):
+    copies = [
+        pltpu.make_async_copy(tokens, tokens_out, sem.at[0]),
+        pltpu.make_async_copy(state, state_out, sem.at[1]),
+    ]
+    for copy in copies:
+        copy.start()
+    for copy in copies:
+        copy.wait()
 
 
 def on_device(
@@ -488,7 +524,10 @@
     layers, mine, groups, width = recurrent_state.shape
     rows, local_d = tokens.shape
     chans = output_weight.shape[1]
-    chunk = rows // n_tp
+    halves, per_block = 2, n_tp // n_dp
+    part_rows = mine // halves
+    chunk = part_rows // per_block
+    blocked = (n_dp, halves, per_block, chunk, local_d)
     hbm = pl.BlockSpec(memory_space=pltpu.HBM)
     dma = pltpu.SemaphoreType.DMA
     in_hbm = lambda a: pltpu.with_memory_space_constraint(a, pltpu.HBM)
@@ -496,7 +535,7 @@
     scratch = [
         pltpu.SMEM(sequence_lengths.shape, sequence_lengths.dtype),
         pltpu.SMEM(discrete_step.shape, discrete_step.dtype),
-        pltpu.VMEM((layers + 1, rows, local_d), BF16),
+        pltpu.VMEM((layers + 1, *blocked), BF16),
         like(norm_weight),
         pltpu.VMEM((layers, local_d, 2 * chans), BF16),
         like(output_weight),
@@ -507,24 +546,24 @@
         like(group_input_matrix),
         like(group_output_matrix),
         like(feedthrough_weight),
-        dma((14,)),
-        pltpu.VMEM((layers, n_dp, mine, 2 * chans), BF16),
-        pltpu.VMEM((layers, n_dp, mine, 2 * chans), BF16),
+        dma((16,)),
+        pltpu.VMEM((layers, halves, n_dp, part_rows, 2 * chans), BF16),
+        pltpu.VMEM((layers, halves, n_dp, part_rows, 2 * chans), BF16),
         dma((1,)),
+        dma((halves,)),
+        pltpu.VMEM((layers, halves, n_dp, 1, 128), F32),
+        pltpu.VMEM((layers, halves, n_dp, 1, 128), F32),
         dma((1,)),
-        pltpu.VMEM((layers, n_dp, 1, 128), F32),
-        pltpu.VMEM((layers, n_dp, 1, 128), F32),
+        dma((halves,)),
+        pltpu.VMEM((layers, halves, n_dp, part_rows, chans), BF16),
         dma((1,)),
+        dma((n_dp + 1,)),
+        pltpu.VMEM((layers, halves, n_tp, chunk, local_d), BF16),
+        pltpu.VMEM((layers, halves, n_tp, chunk, local_d), BF16),
         dma((1,)),
-        pltpu.VMEM((layers, n_dp, mine, chans), BF16),
+        dma((halves, 3)),
         dma((1,)),
-        dma((n_dp,)),
-        pltpu.VMEM((layers, n_tp, chunk, local_d), BF16),
-        pltpu.VMEM((layers, n_tp, chunk, local_d), BF16),
-        dma((1,)),
-        dma((n_tp,)),
-        dma((1,)),
-        dma((n_tp,)),
+        dma((halves, 5)),
         pltpu.VMEM((mine, groups, width), F32),
         pltpu.VMEM((layers, mine, groups, width), F32),
         pltpu.VMEM((layers, chans, width), BF16),
@@ -533,10 +572,10 @@
         pltpu.VMEM((layers, mine, chans), F32),
         pltpu.SemaphoreType.REGULAR,
     ]
-    return pl.pallas_call(
+    tokens_out, state_out = pl.pallas_call(
         functools.partial(kernel, n_dp, n_tp, n_dp * local_d),
         out_shape=(
-            jax.ShapeDtypeStruct(tokens.shape, tokens.dtype),
+            jax.ShapeDtypeStruct(blocked, tokens.dtype),
             jax.ShapeDtypeStruct(recurrent_state.shape, recurrent_state.dtype),
         ),
         in_specs=[hbm] * 14,
@@ -546,7 +585,7 @@
     )(
         in_hbm(sequence_lengths),
         in_hbm(discrete_step),
-        in_hbm(tokens),
+        in_hbm(tokens.reshape(blocked)),
         in_hbm(norm_weight),
         in_hbm(input_weight),
         in_hbm(gate_weight),
@@ -560,6 +599,18 @@
         in_hbm(output_weight),
     )
 
+    vmem = pl.BlockSpec(memory_space=pltpu.VMEM)
+    return pl.pallas_call(
+        write_out,
+        out_shape=(
+            jax.ShapeDtypeStruct(tokens.shape, tokens.dtype),
+            jax.ShapeDtypeStruct(recurrent_state.shape, recurrent_state.dtype),
+        ),
+        in_specs=[vmem, vmem],
+        out_specs=(hbm, hbm),
+        scratch_shapes=[dma((2,))],
+        compiler_params=pltpu.CompilerParams(vmem_limit_bytes=16 * 2**20),
+    )(tokens_out.reshape(tokens.shape), state_out)
 
 def solution(mesh):
     in_specs = (

time: 84.8 us -> 82.8 us (0.976)
  local copies, waits for them, and re-layouts: 1.41 us -> 0 us
  Pallas kernels: 82.7 us -> 81.8 us
    pallas_call x1, Pallas kernels: 82.7 us -> 81 us  [on_device(): pl.pallas_call(functools.partial(kernel, n_dp, n_tp, n_dp * local_d), out...]
    unnamed x2 -> x0, local copies, waits for them, and re-layouts: 1.41 us -> none
where the time goes in v6:
time: 82.8 us; the launch traced here: 82.5 us
  Pallas kernels  81.8 us (99%)
    pallas_call x1, Pallas kernels, on_device(): pl.pallas_call(functools.partial(kernel, n_dp, n_tp, n_dp * local_d), out...  81 us

profile of v6, /device:TPU:40, one launch (start us, length us, event | category | flops | bytes accessed | tf_op | source)
XLA Modules:
  0.0 82.5 jit_solution(9748626498264733733)
XLA Ops:
  0.6 81.0 %shard_map.149 = (bf16[8,2,2,8,512]{4,3,2,1,0:T(8,128)(2,1)S(1)}, f32[2,32,8,128]{3,2,1,0:T(8,128)S(1)}) custom-call(s32[32]{0:T(128)} %lengths_hbm.1, f32[2,8]{1,0:T(2,128)} %step_hbm.1, bf16[8,2,2,8,512]{4,3,2,1,0:T(8,128)(2,1)} %bitcast.3, f32[2,512]{1,0:T(2,128)} %norm_hbm.1, bf16[2,512,128]{2,1,0:T(8,128)(2,1)} %w_in_hbm.1, ...), custom_call_target="tpu_custom_call" | custom-call | tf_op jit(solution)/shard_map/pallas_call | solution.py:575
  81.7 0.8 shard_map.150

commit v7 on v6

--- a/solution.py
+++ b/solution.py
@@ -472,12 +472,12 @@
         u_f = [mix(layer, h) for h in both]
         for h in both:
             project(layer, h)
-        for h in both:
-            new_state(layer, h, u_f[h])
         if layer == 0:
             pl.semaphore_wait(relay, 2)
         for h in both:
             sum_at_hubs(layer, h)
+        for h in both:
+            new_state(layer, h, u_f[h])
         for h in both:
             own_chunk(layer, h)
         for h in both:

time: 82.8 us -> 82.7 us (level)
  no operation moved by 1% of the time
where the time goes in v7:
time: 82.7 us; the launch traced here: 82.5 us
  Pallas kernels  81.8 us (99%)
    pallas_call x1, Pallas kernels, on_device(): pl.pallas_call(functools.partial(kernel, n_dp, n_tp, n_dp * local_d), out...  81 us

profile of v7, /device:TPU:40, one launch (start us, length us, event | category | flops | bytes accessed | tf_op | source)
XLA Modules:
  0.0 82.5 jit_solution(1700439515297214063)
XLA Ops:
  0.6 81.0 %shard_map.149 = (bf16[8,2,2,8,512]{4,3,2,1,0:T(8,128)(2,1)S(1)}, f32[2,32,8,128]{3,2,1,0:T(8,128)S(1)}) custom-call(s32[32]{0:T(128)} %lengths_hbm.1, f32[2,8]{1,0:T(2,128)} %step_hbm.1, bf16[8,2,2,8,512]{4,3,2,1,0:T(8,128)(2,1)} %bitcast.3, f32[2,512]{1,0:T(2,128)} %norm_hbm.1, bf16[2,512,128]{2,1,0:T(8,128)(2,1)} %w_in_hbm.1, ...), custom_call_target="tpu_custom_call" | custom-call | tf_op jit(solution)/shard_map/pallas_call | solution.py:575
  81.7 0.8 shard_map.150
